TPU v7x, 32 devices: a whole 2x2x4 slice. The times are simulated.
32 devices in a mesh: fs: 16 (over z, y, x), tp: 2 (over core).
Axes of the slice: x: 2, y: 2, z: 4, core: 2. Of those that a mesh axis runs over, the one named last changes fastest.
Arguments:
- tokens: bfloat16 [4096, 2048], P('fs', 'tp'), may hold values from -6 to 6
- mixer_norm_gain: bfloat16 [2048], replicated, may hold values from 0.099609375 to 1.8984375
- recurrence_branch_weight: bfloat16 [2048, 1024], P('fs', 'tp'), may hold values from -0.125 to 0.125
- output_gate_projection: bfloat16 [2048, 1024], P('fs', 'tp'), may hold values from -0.125 to 0.125
- recurrence_conv_taps: bfloat16 [4, 1024], P(None, 'tp'), may hold values from -3 to 3
- recurrence_gate_map: bfloat16 [16, 64, 64], P('tp'), may hold values from -0.75 to 0.75
- input_gate_map: bfloat16 [16, 64, 64], P('tp'), may hold values from -0.75 to 0.75
- channel_decay_rate: float32 [1024], P('tp'), may hold values from 0.001 to 0.03
- position_log_decay: float32 [4096, 1024], P('fs', 'tp'), may hold values from -0.69 to 0
- mixer_output_weight: bfloat16 [1024, 2048], P('tp', 'fs'), may hold values from -0.75 to 0.75
- feedforward_norm_gain: bfloat16 [2048], replicated, may hold values from 0.099609375 to 1.8984375
- gate_up_weight: bfloat16 [2048, 5632], P('fs', 'tp'), may hold values from -0.125 to 0.125
- value_up_weight: bfloat16 [2048, 5632], P('fs', 'tp'), may hold values from -0.125 to 0.125
- gate_conv_taps: bfloat16 [3, 5632], P(None, 'tp'), may hold values from -3 to 3
- value_conv_taps: bfloat16 [3, 5632], P(None, 'tp'), may hold values from -3 to 3
- down_projection_weight: bfloat16 [5632, 2048], P('tp', 'fs'), may hold values from -0.15625 to 0.15625
Outputs:
- result: bfloat16 [4096, 2048], P('fs', 'tp')
All inputs are finite; a program needn't handle non-finite values.
Results may differ from a plain program's by a relative error of at most 0.024.
Values may be sent and summed in bfloat16 or wider, within the bound.
A program may use at most 128 MiB of HBM per device.

v0:
```python
import functools

import jax
import jax.numpy as jnp
from jax import lax
from jax.experimental import pallas as pl
from jax.experimental.pallas import tpu as pltpu
from jax.sharding import PartitionSpec as P

SEQ_LEN = 64


EPS = 1e-06
DECAY_RATE_GAIN = 8.0


def rms_normed(values, gain):
    wide = values.astype(jnp.float32)
    factor = lax.rsqrt(jnp.mean(wide * wide, axis=-1, keepdims=True) + EPS)
    return (wide * factor * gain.astype(jnp.float32)).astype(jnp.bfloat16)


def causal_conv(values, kernel):
    width = kernel.shape[0]
    row_count, channels = values.shape
    grouped = values.astype(jnp.float32).reshape(row_count // SEQ_LEN, SEQ_LEN, channels)
    padded = jnp.pad(grouped, ((0, 0), (width - 1, 0), (0, 0)))
    summed = padded[:, 0:SEQ_LEN] * kernel[0].astype(jnp.float32)
    for offset in range(1, width):
        summed = summed + padded[:, offset : offset + SEQ_LEN] * kernel[offset].astype(jnp.float32)
    return summed.reshape(row_count, channels)


def combine(left, right):
    first_a, first_b = left
    second_a, second_b = right
    return (first_a * second_a, second_a * first_b + second_b)


def pair_folder(normed, pieces):
    return (
        jnp.dot(normed, pieces[0], preferred_element_type=jnp.float32),
        jnp.dot(normed, pieces[1], preferred_element_type=jnp.float32),
    )


def gathered_layer(
    tokens,
    mixer_norm_gain,
    recurrence_branch_weight,
    output_gate_projection,
    recurrence_conv_taps,
    recurrence_gate_map,
    input_gate_map,
    channel_decay_rate,
    position_log_decay,
    mixer_output_weight,
    feedforward_norm_gain,
    gate_up_weight,
    value_up_weight,
    gate_conv_taps,
    value_conv_taps,
    down_projection_weight,
):
    row_count = tokens.shape[0]
    local_width = recurrence_branch_weight.shape[1]
    local_heads = recurrence_gate_map.shape[0]
    head_size = recurrence_gate_map.shape[1]
    whole_rows = lax.all_gather(tokens, "tp", axis=1, tiled=True)
    normed = rms_normed(whole_rows, mixer_norm_gain)
    branch_sum, outgate_sum = pair_folder(
        normed,
        (
            lax.all_gather(recurrence_branch_weight, "fs", axis=0, tiled=True),
            lax.all_gather(output_gate_projection, "fs", axis=0, tiled=True),
        ),
    )
    branch = branch_sum.astype(jnp.bfloat16)
    outgate = outgate_sum.astype(jnp.bfloat16)
    conv = causal_conv(branch, recurrence_conv_taps).astype(jnp.bfloat16)
    grouped = conv.reshape(row_count, local_heads, head_size)
    recurrence_scan = jax.nn.sigmoid(
        jnp.einsum(
            "rhi,hij->rhj", grouped, recurrence_gate_map, preferred_element_type=jnp.float32
        ).reshape(row_count, local_width)
    )
    inner = jax.nn.sigmoid(
        jnp.einsum(
            "rhi,hij->rhj", grouped, input_gate_map, preferred_element_type=jnp.float32
        ).reshape(row_count, local_width)
    )
    log_alpha = (
        -DECAY_RATE_GAIN * recurrence_scan * channel_decay_rate[None, :] + position_log_decay
    )
    drive = jnp.sqrt(-jnp.expm1(2.0 * log_alpha)) * inner * conv.astype(jnp.float32)
    shape3 = (row_count // SEQ_LEN, SEQ_LEN, local_width)
    unused, state = lax.associative_scan(
        combine, (jnp.exp(log_alpha).reshape(shape3), drive.reshape(shape3)), axis=1
    )
    state = state.reshape(row_count, local_width)
    mixed = (state * jax.nn.gelu(outgate.astype(jnp.float32))).astype(jnp.bfloat16)
    mixer_terms = jnp.dot(
        mixed,
        lax.all_gather(mixer_output_weight, "fs", axis=1, tiled=True),
        preferred_element_type=jnp.float32,
    )
    mixer_terms = mixer_terms.astype(jnp.bfloat16).astype(jnp.float32)
    mixer_whole = lax.psum(mixer_terms.astype(jnp.bfloat16), "tp").astype(jnp.float32)
    whole_after = (whole_rows.astype(jnp.float32) + mixer_whole).astype(jnp.bfloat16)
    normed2 = rms_normed(whole_after, feedforward_norm_gain)
    gate_whole, value_whole = (
        lax.all_gather(gate_up_weight, "fs", axis=0, tiled=True),
        lax.all_gather(value_up_weight, "fs", axis=0, tiled=True),
    )
    gate_sum = jnp.dot(normed2, gate_whole, preferred_element_type=jnp.float32)
    value_sum = jnp.dot(normed2, value_whole, preferred_element_type=jnp.float32)
    gate_half = gate_sum.astype(jnp.bfloat16)
    value_half = value_sum.astype(jnp.bfloat16)
    hidden = (
        jax.nn.silu(causal_conv(gate_half, gate_conv_taps))
        * causal_conv(value_half, value_conv_taps)
    ).astype(jnp.bfloat16)
    channel_terms = jnp.dot(
        hidden,
        lax.all_gather(down_projection_weight, "fs", axis=1, tiled=True),
        preferred_element_type=jnp.float32,
    )
    channel_terms = channel_terms.astype(jnp.bfloat16).astype(jnp.float32)
    channel_share = lax.psum_scatter(
        channel_terms.astype(jnp.bfloat16), "tp", scatter_dimension=1, tiled=True
    ).astype(jnp.float32)
    share_width = channel_share.shape[1]
    residual_share = lax.dynamic_slice_in_dim(
        whole_after, lax.axis_index("tp") * share_width, share_width, 1
    )
    return (residual_share.astype(jnp.float32) + channel_share).astype(jnp.bfloat16)


PLANE = 4
LAYERS = 4
LANES = 128
ANY = pl.BlockSpec(memory_space=pl.ANY)
VMEM = pl.BlockSpec(memory_space=pltpu.VMEM)
F32, BF16 = jnp.float32, jnp.bfloat16
N_SMALL, N_BIG = 3, 5


def hop(src, dst, send, recv, target):
    return pltpu.make_async_remote_copy(
        src_ref=src,
        dst_ref=dst,
        send_sem=send,
        recv_sem=recv,
        device_id=target,
        device_id_type=pl.DeviceIdType.MESH,
    )


def greet(targets):
    barrier = pltpu.get_barrier_semaphore()
    for target in targets:
        pl.semaphore_signal(
            barrier, inc=1, device_id=target, device_id_type=pl.DeviceIdType.MESH
        )
    pl.semaphore_wait(barrier, len(targets))


def span(index, size):
    return pl.ds(pl.multiple_of(index * size, size), size)


def row_blocks(whole, deep, columns):
    def at(f, part=None):
        if part is None:
            return whole.at[span(f, deep), columns]
        return whole.at[span(f * 2 + part, deep // 2), columns]

    return at


def column_blocks(whole, rows, wide):
    def at(f, part=None):
        if part is None:
            return whole.at[pl.ds(0, rows), span(f, wide)]
        return whole.at[pl.ds(part * (rows // 2), rows // 2), span(f, wide)]

    return at


def position(shape):
    return lax.broadcasted_iota(jnp.int32, shape, 0) % SEQ_LEN


def shifted(values, distance, place, fill):
    return jnp.where(place >= distance, pltpu.roll(values, distance, 0), fill)


def rows_conv(values, taps, width, place):
    summed = shifted(values, width - 1, place, 0.0) * taps[0:1, :]
    for j in range(1, width - 1):
        summed = summed + shifted(values, width - 1 - j, place, 0.0) * taps[j : j + 1, :]
    return summed + values * taps[width - 1 : width, :]


def negative_expm1(x):
    near = 1.0 + x * (1.0 / 8.0)
    for n in range(7, 1, -1):
        near = 1.0 + x * (1.0 / n) * near
    return jnp.where(jnp.abs(x) < 0.4, -x * near, 1.0 - jnp.exp(x))


def normed_rows(values, gain):
    factor = lax.rsqrt(jnp.mean(values * values, axis=-1, keepdims=True) + EPS)
    return (values * factor * gain).astype(BF16)


def gelu(x):
    return 0.5 * x * (1.0 + jnp.tanh(0.7978845608028654 * (x + 0.044715 * (x * x * x))))


def layer_kernel(
    tok, gain1, rb, og, ctaps, rmap, imap, rate, pld, mo, gain2, gup, vup, gtaps, vtaps, dn,
    out,
    whole_tok, bo_all, mo_all, gup_v, vup_v, stage, gu_all, dn_all, taps, gmap, pld_v,
    normed, mixed, mine, theirs, after, n2, hidden, give, keep, pair, paired, own_part, arrive,
    send, recv, z_send, local, tok_sem, swap_send, swap_recv, n2_send, n2_recv,
    core_send, core_recv, pair_send, pair_recv, back_send, back_recv,
):
    fs, tp = lax.axis_index("fs"), lax.axis_index("tp")
    z, p = fs // PLANE, fs % PLANE
    y, x = p // 2, p % 2
    px, py = y * 2 + 1 - x, (1 - y) * 2 + x
    inner = ((z + 1) // 2) % 2
    layer = (z, z + 1 - 2 * (z % 2), 2 - z // 2, 3 - 3 * (z // 2))
    lands = (0, 1, 3 - inner, 3 - inner)
    line = [(zz * PLANE + p, tp) for zz in layer]
    x_target, y_target = (z * PLANE + px, tp), (z * PLANE + py, tp)
    core_target = (fs, 1 - tp)
    greet(line[1:] + [x_target, y_target, core_target])

    rows, half = tok.shape
    deep, local_width = rb.shape
    wide = mo.shape[1]
    units = dn.shape[0] // LAYERS
    full, rest = units // LANES, units % LANES
    cw = gmap.shape[1]
    heads, head = rmap.shape[:2]
    per = cw // head

    arrays = (
        (row_blocks(bo_all, deep, pl.ds(0, local_width)), rb),
        (row_blocks(bo_all, deep, pl.ds(local_width, local_width)), og),
        (column_blocks(mo_all, mo.shape[0], wide), mo),
        (row_blocks(gu_all, deep, slice(None)), None),
        (column_blocks(dn_all, units, wide), None),
    )

    def piece(a, zz):
        if a < N_SMALL:
            return arrays[a][1]
        return stage.at[zz] if a == 3 else dn.at[span(zz, units), :]

    pending = []
    inner_pending = []

    copy = hop(tok, whole_tok.at[:, span(tp, half)], tok_sem.at[0], tok_sem.at[1], core_target)
    copy.start()
    tok_copy = copy

    def z_hop(a, source, f, slot, land, to):
        return hop(source, arrays[a][0](f), z_send.at[a, slot], recv.at[a, 0, land], line[to])

    def sides(a, k):
        at = arrays[a][0]
        f = layer[k] * PLANE + p
        source = piece(a, z) if k == 0 else at(f)
        for kind, target in ((1, x_target), (2, y_target)):
            c = hop(source, at(f), send.at[a, kind, k], recv.at[a, kind, k], target)
            c.start()
            pending.append(c)

    def corners(a, k):
        at = arrays[a][0]
        base = layer[k] * PLANE
        for kind, part, owner, target in ((1, 0, px, y_target), (2, 1, py, x_target)):
            whole = at(base + owner)
            hop(whole, whole, send.at[a, kind, k], recv.at[a, kind, k], target).wait_recv()
            block = at(base + owner, part)
            c = hop(block, block, send.at[a, kind + 2, k], recv.at[a, kind + 2, k], target)
            c.start()
            pending.append(c)

    def corners_done(a, k):
        at = arrays[a][0]
        corner = layer[k] * PLANE + (PLANE - 1 - p)
        for kind, part, target in ((1, 0, y_target), (2, 1, x_target)):
            block = at(corner, part)
            hop(block, block, send.at[a, kind + 2, k], recv.at[a, kind + 2, k], target).wait_recv()

    def z_done(a, k):
        block = arrays[a][0](layer[k] * PLANE + p)
        hop(block, block, z_send.at[a, 0], recv.at[a, 0, k], line[k]).wait_recv()

    @pl.when(inner == 1)
    def _():
        for a in range(N_SMALL):
            z_hop(a, piece(a, z), fs, 1, 2, 2).start()

    for a in range(N_SMALL):
        c = z_hop(a, piece(a, z), fs, 0, 1, 1)
        c.start()
        pending.append(c)
    inner_pending += [(a, 1) for a in range(N_SMALL)]
    for a in range(N_SMALL):
        sides(a, 0)

    own = [
        pltpu.make_async_copy(gup, gup_v, local.at[0]),
        pltpu.make_async_copy(vup, vup_v, local.at[1]),
        pltpu.make_async_copy(tok, whole_tok.at[:, span(tp, half)], local.at[2]),
        pltpu.make_async_copy(pld, pld_v, local.at[3]),
        pltpu.make_async_copy(rb, arrays[0][0](fs), local.at[4]),
        pltpu.make_async_copy(og, arrays[1][0](fs), local.at[5]),
        pltpu.make_async_copy(mo, arrays[2][0](fs), local.at[6]),
        pltpu.make_async_copy(piece(4, z), arrays[4][0](fs), local.at[7]),
    ]
    for c in own:
        c.start()

    own[0].wait()
    own[1].wait()

    def arrange(gate, value, zz, store):
        for j in range(full):
            at = zz * units + j * LANES
            store(2 * j * LANES, gate[:, at : at + LANES])
            store((2 * j + 1) * LANES, value[:, at : at + LANES])
        if rest:
            at = zz * units + full * LANES
            store(2 * full * LANES, gate[:, at : at + rest])
            store(2 * full * LANES + rest, value[:, at : at + rest])

    for zz in range(LAYERS):

        def put(at, v, zz=zz):
            stage[zz, :, at : at + v.shape[1]] = v

        def put_taps(at, v, zz=zz):
            taps[zz, 0 : v.shape[0], at : at + v.shape[1]] = v.astype(F32)

        arrange(gup_v, vup_v, zz, put)
        arrange(gtaps, vtaps, zz, put_taps)
    gu_all[span(fs, deep), :] = stage[z]
    dn_all[units:, :] = jnp.zeros((dn_all.shape[0] - units, dn_all.shape[1]), BF16)
    gmap[...] = jnp.zeros(gmap.shape, BF16)
    for c in range(heads // per):
        for h in range(per):
            r = slice(h * head, (h + 1) * head)
            gmap[c, r, h * head : (h + 1) * head] = rmap[c * per + h]
            gmap[c, r, cw + h * head : cw + (h + 1) * head] = imap[c * per + h]

    def relay(k, to, land, slot):
        @pl.when(inner == 1)
        def _():
            for a in range(N_SMALL):
                f = layer[k] * PLANE + p
                z_hop(a, arrays[a][0](f), f, slot, land, to).start()

        inner_pending.extend((a, slot) for a in range(N_SMALL))

    for k, to, land in ((1, 2, 3), (2, 1, 2), (3, 1, 3)):
        for a in range(N_SMALL):
            z_done(a, k)
        relay(k, to, land, k + 1)
        for a in range(N_SMALL):
            sides(a, k)
        for a in range(N_SMALL):
            corners(a, k - 1)
    for a in range(N_SMALL, N_BIG):
        for k in range(1, LAYERS):
            c = z_hop(a, piece(a, layer[k]), fs, k, lands[k], k)
            c.start()
            pending.append(c)
    for a in range(N_SMALL):
        corners(a, LAYERS - 1)
    sides(3, 0)
    z_done(3, 1)
    sides(3, 1)

    tok_copy.wait_recv()
    own[2].wait()
    wide_tok = whole_tok[...].astype(F32)
    normed[...] = normed_rows(wide_tok, gain1[...].astype(F32))
    for c in own[3:]:
        c.wait()
    for k in range(LAYERS):
        for a in range(N_SMALL):
            corners_done(a, k)

    def mixer_chunk(c, _):
        at = span(c, cw)
        place = position((rows, cw))
        branch = jnp.dot(normed[...], bo_all[:, at], preferred_element_type=F32)
        branch = branch.astype(BF16).astype(F32)
        conv = rows_conv(branch, ctaps[:, at].astype(F32), ctaps.shape[0], place).astype(BF16)
        gates = jax.nn.sigmoid(jnp.dot(conv, gmap[c], preferred_element_type=F32))
        la = -DECAY_RATE_GAIN * gates[:, :cw] * rate[:, at] + pld_v[:, at]
        d = jnp.sqrt(negative_expm1(2.0 * la)) * gates[:, cw:] * conv.astype(F32)
        a = jnp.exp(la)
        step = 1
        while step < SEQ_LEN:
            d = a * shifted(d, step, place, 0.0) + d
            if step * 2 < SEQ_LEN:
                a = a * shifted(a, step, place, 1.0)
            step *= 2
        outgate = jnp.dot(
            normed[...],
            bo_all[:, pl.ds(pl.multiple_of(local_width + c * cw, cw), cw)],
            preferred_element_type=F32,
        )
        outgate = outgate.astype(BF16).astype(F32)
        mixed[:, at] = (d * gelu(outgate)).astype(BF16)
        return 0

    lax.fori_loop(0, local_width // cw, mixer_chunk, 0)
    z_done(3, 2)
    sides(3, 2)
    mix_wide = mine.shape[2]
    swaps = []
    for c in range(mine.shape[0]):
        mine[c] = jnp.dot(
            mixed[...], mo_all[:, c * mix_wide : (c + 1) * mix_wide], preferred_element_type=F32
        ).astype(BF16)
        s = hop(mine.at[c], theirs.at[c], swap_send.at[c], swap_recv.at[c], core_target)
        s.start()
        swaps.append(s)
    z_done(3, 3)
    sides(3, 3)
    square = jnp.zeros((rows, 1), F32)
    for c in range(mine.shape[0]):
        at = slice(c * mix_wide, (c + 1) * mix_wide)
        swaps[c].wait_recv()
        both = mine[c].astype(F32) + theirs[c].astype(F32)
        total = (whole_tok[:, at].astype(F32) + both).astype(BF16)
        after[:, at] = total
        total = total.astype(F32)
        square = square + jnp.sum(total * total, axis=-1, keepdims=True)
    factor = lax.rsqrt(square * (1.0 / after.shape[1]) + EPS)
    n2[0] = (after[...].astype(F32) * factor * gain2[...].astype(F32)).astype(BF16)

    mine_half = span(tp, half)

    def rows_hop(k, land, slot, to):
        return hop(
            n2.at[k, :, mine_half], n2.at[land, :, mine_half], n2_send.at[slot], n2_recv.at[land], line[to]
        )

    @pl.when(inner == 1)
    def _():
        rows_hop(0, 2, 1, 2).start()

    c = rows_hop(0, 1, 0, 1)
    c.start()
    pending.append(c)
    across = {}

    def rows_arrived(k, to, land):
        rows_hop(k, k, 0, 1).wait_recv()

        @pl.when(inner == 1)
        def _():
            rows_hop(k, land, k + 1, to).start()

        block = n2.at[k, :, mine_half]
        across[k] = hop(block, block, core_send.at[k], core_recv.at[k], core_target)
        across[k].start()

    for k in range(LAYERS):
        corners(3, k)
    dn_order = (0, 2, 1, 3)
    sides(4, 0)
    for k in dn_order[1:]:
        z_done(4, k)
        sides(4, k)
    rows_arrived(1, 2, 3)
    rows_arrived(2, 1, 2)

    def up(k):
        place = position((rows, 4 * LANES))
        layer_taps = taps.at[z]
        width = gtaps.shape[0]
        j = 0
        while j < 2 * full * LANES:
            n = min(4 * LANES, 2 * full * LANES - j)
            s = jnp.dot(n2[k], gu_all[:, j : j + n], preferred_element_type=F32)
            s = rows_conv(s.astype(BF16).astype(F32), layer_taps[0:width, j : j + n], width, place[:, :n])
            for i in range(0, n, 2 * LANES):
                g, v = s[:, i : i + LANES], s[:, i + LANES : i + 2 * LANES]
                h = (j + i) // 2
                hidden[k, :, h : h + LANES] = (g * jax.nn.sigmoid(g) * v).astype(BF16)
            j += n
        if rest:
            s = jnp.dot(n2[k], gu_all[:, j:], preferred_element_type=F32)
            s = rows_conv(s.astype(BF16).astype(F32), layer_taps[0:width, j:], width, place[:, :LANES])
            h = s * jax.nn.sigmoid(s) * pltpu.roll(s, rest, 1)
            lane = lax.broadcasted_iota(jnp.int32, h.shape, 1)
            hidden[k, :, full * LANES : (full + 1) * LANES] = jnp.where(lane < rest, h, 0.0).astype(BF16)

    def up_step(k, _):
        up(k)
        return 0

    for k in range(LAYERS):
        corners_done(3, k)
    lax.fori_loop(0, 1, up_step, 0)
    corners(4, 0)
    corners(4, 2)
    across[1].wait_recv()
    across[2].wait_recv()
    rows_arrived(3, 1, 3)
    lax.fori_loop(1, 3, up_step, 0)
    corners(4, 1)
    corners(4, 3)
    across[3].wait_recv()
    lax.fori_loop(3, 4, up_step, 0)

    turn = (tp + z // 2) % 2
    chunk = PLANE * wide
    backs = []
    for i in range(LAYERS // 2):
        first, second = layer[i], layer[i + 2]
        kept = first * (1 - turn) + second * turn
        given = first * turn + second * (1 - turn)
        corners_done(4, i)
        corners_done(4, i + 2)

        def give_step(k, _):
            give[i, k] = jnp.dot(
                hidden[k], dn_all[:, span(given, chunk)], preferred_element_type=F32
            ).astype(BF16)
            return 0

        def keep_step(k, _):
            keep[k] = jnp.dot(
                hidden[k], dn_all[:, span(kept, chunk)], preferred_element_type=F32
            ).astype(BF16)
            return 0

        lax.fori_loop(0, LAYERS, give_step, 0)
        s = hop(give.at[i], pair.at[i], pair_send.at[i], pair_recv.at[i], core_target)
        s.start()
        pending.append(s)
        lax.fori_loop(0, LAYERS, keep_step, 0)
        s.wait_recv()
        place_at = span(kept % 2, chunk)

        def pair_step(k, _):
            paired[i, k] = (keep[k].astype(F32) + pair[i, k].astype(F32)).astype(BF16)
            return 0

        lax.fori_loop(0, LAYERS, pair_step, 0)
        own_part[:, place_at] = paired[i, 0]
        for k in range(1, LAYERS):
            c = hop(
                paired.at[i, k], arrive.at[lands[k] - 1, :, place_at],
                back_send.at[i, k], back_recv.at[i, lands[k]], line[k],
            )
            c.start()
            pending.append(c)
            block = arrive.at[k - 1, :, place_at]
            backs.append(hop(paired.at[i, k], block, back_send.at[i, k], back_recv.at[i, k], line[k]))

    for c in backs:
        c.wait_recv()
    total = own_part[...].astype(F32)
    for k in range(LAYERS - 1):
        total = total + arrive[k].astype(F32)
    out[...] = (after[:, mine_half].astype(F32) + total).astype(BF16)

    for c in pending + swaps + list(across.values()) + [tok_copy]:
        c.wait_send()

    @pl.when(inner == 1)
    def _():
        for a, slot in inner_pending:
            z_hop(a, arrays[a][0](fs), fs, slot, 0, 1).wait_send()
        for slot in range(1, LAYERS + 1):
            rows_hop(0, 0, slot, 1).wait_send()


def fused_layer(
    tokens,
    mixer_norm_gain,
    recurrence_branch_weight,
    output_gate_projection,
    recurrence_conv_taps,
    recurrence_gate_map,
    input_gate_map,
    channel_decay_rate,
    position_log_decay,
    mixer_output_weight,
    feedforward_norm_gain,
    gate_up_weight,
    value_up_weight,
    gate_conv_taps,
    value_conv_taps,
    down_projection_weight,
):
    rows, half = tokens.shape
    deep, local_width = recurrence_branch_weight.shape
    wide = mixer_output_weight.shape[1]
    n_fs = LAYERS * PLANE
    features = 2 * half
    local_units = gate_up_weight.shape[1]
    units = local_units // LAYERS
    padded = -(-units // (2 * LANES)) * 2 * LANES
    head = recurrence_gate_map.shape[1]
    cw = min(local_width, 4 * head)
    chunk = PLANE * wide
    dma = pltpu.SemaphoreType.DMA
    scratch = [
        pltpu.VMEM((rows, features), BF16),
        pltpu.VMEM((n_fs * deep, 2 * local_width), BF16),
        pltpu.VMEM((local_width, n_fs * wide), BF16),
        pltpu.VMEM((deep, local_units), BF16),
        pltpu.VMEM((deep, local_units), BF16),
        pltpu.VMEM((LAYERS, deep, 2 * units), BF16),
        pltpu.VMEM((n_fs * deep, 2 * units), BF16),
        pltpu.VMEM((padded, n_fs * wide), BF16),
        pltpu.VMEM((LAYERS, 8, 2 * units), F32),
        pltpu.VMEM((local_width // cw, cw, 2 * cw), BF16),
        pltpu.VMEM((rows, local_width), F32),
        pltpu.VMEM((rows, features), BF16),
        pltpu.VMEM((rows, local_width), BF16),
        pltpu.VMEM((LAYERS, rows, chunk), BF16),
        pltpu.VMEM((LAYERS, rows, chunk), BF16),
        pltpu.VMEM((rows, features), BF16),
        pltpu.VMEM((LAYERS, rows, features), BF16),
        pltpu.VMEM((LAYERS, rows, padded), BF16),
        pltpu.VMEM((2, LAYERS, rows, chunk), BF16),
        pltpu.VMEM((LAYERS, rows, chunk), BF16),
        pltpu.VMEM((2, LAYERS, rows, chunk), BF16),
        pltpu.VMEM((2, LAYERS, rows, chunk), BF16),
        pltpu.VMEM((rows, half), BF16),
        pltpu.VMEM((LAYERS - 1, rows, half), BF16),
        dma((N_BIG, 5, LAYERS)),
        dma((N_BIG, 5, LAYERS)),
        dma((N_BIG, LAYERS + 1)),
        dma((8,)),
        dma((2,)),
        dma((LAYERS,)),
        dma((LAYERS,)),
        dma((LAYERS + 1,)),
        dma((LAYERS,)),
        dma((LAYERS,)),
        dma((LAYERS,)),
        dma((2,)),
        dma((2,)),
        dma((2, LAYERS)),
        dma((2, LAYERS)),
    ]
    return pl.pallas_call(
        layer_kernel,
        out_shape=jax.ShapeDtypeStruct((rows, half), BF16),
        in_specs=[ANY, VMEM, ANY, ANY, VMEM, VMEM, VMEM, VMEM, ANY, ANY, VMEM, ANY, ANY, VMEM, VMEM, ANY],
        out_specs=VMEM,
        scratch_shapes=scratch,
        compiler_params=pltpu.CompilerParams(
            collective_id=0, has_side_effects=True, vmem_limit_bytes=62 * 2**20
        ),
        name="layer",
    )(
        tokens,
        mixer_norm_gain.reshape(1, -1),
        recurrence_branch_weight,
        output_gate_projection,
        recurrence_conv_taps,
        recurrence_gate_map,
        input_gate_map,
        channel_decay_rate.reshape(1, -1),
        position_log_decay,
        mixer_output_weight,
        feedforward_norm_gain.reshape(1, -1),
        gate_up_weight,
        value_up_weight,
        gate_conv_taps,
        value_conv_taps,
        down_projection_weight,
    )


def solution(mesh):
    placed = (
        P("fs", "tp"),
        P(),
        P("fs", "tp"),
        P("fs", "tp"),
        P(None, "tp"),
        P("tp", None, None),
        P("tp", None, None),
        P("tp"),
        P("fs", "tp"),
        P("tp", "fs"),
        P(),
        P("fs", "tp"),
        P("fs", "tp"),
        P(None, "tp"),
        P(None, "tp"),
        P("tp", "fs"),
    )
    fused = mesh.shape["tp"] == 2 and mesh.shape["fs"] == LAYERS * PLANE
    body = fused_layer if fused else gathered_layer
    return jax.shard_map(
        body, mesh=mesh, in_specs=placed, out_specs=P("fs", "tp"), check_vma=False
    )
```

profile of v0, /device:TPU:0, one launch (start us, length us, event | category | flops | bytes accessed | tf_op | source)
XLA Modules:
  0.0 185.2 jit_solution(8159546820055239361)
XLA Ops:
  0.0 0.0 copy-start
  0.0 1.3 reshape.9.gain1
  1.3 0.0 copy-done
  1.3 0.6 reshape.11.gain2
  1.9 181.4 %layer.1 = bf16[256,1024]{1,0:T(8,128)(2,1)} custom-call(bf16[256,1024]{1,0:T(8,128)(2,1)} %tok.1, bf16[1,2048]{1,0:T(2,128)(2,1)} %reshape.9.gain1, bf16[128,512]{1,0:T(8,128)(2,1)} %rb.1, bf16[128,512]{1,0:T(8,128)(2,1)} %og.1, bf16[4,512]{1,0:T(4,128)(2,1)} %ctaps.1, bf16[8,64,64]{2,1,0:T(8,128)(2,1)} %rmap.1, bf16[8,64,64]{2,1,0:T(8,128)(2,1)} %imap.1, ...), custom_call_target="tpu_custom_call" | custom-call | tf_op jit(solution)/shard_map/layer/pallas_call | solution.py:662
  183.4 1.9 %copy.18 = bf16[256,1024]{1,0:T(8,128)(2,1)} copy(bf16[256,1024]{1,0:T(8,128)(2,1)} %layer.1) | data formatting | bytes 1048576
Async XLA Ops:
  0.0 1.3 copy-start
where the time goes:
time: 185 us
  Pallas kernels  181 us (98%)
  local copies, waits for them, and re-layouts  3.77 us (2%)
    pallas_call x1, Pallas kernels, fused_layer(): pl.pallas_call(layer_kernel, out_shape=jax.ShapeDtypeStruct((rows, half),...  181 us

commit v1 on v0

--- a/solution.py
+++ b/solution.py
@@ -222,9 +222,9 @@
     tok, gain1, rb, og, ctaps, rmap, imap, rate, pld, mo, gain2, gup, vup, gtaps, vtaps, dn,
     out,
     whole_tok, bo_all, mo_all, gup_v, vup_v, stage, gu_all, dn_all, taps, gmap, pld_v,
-    normed, mixed, mine, theirs, after, n2, hidden, give, keep, pair, paired, own_part, arrive,
+    normed, mixed, mine, theirs, after, n2, hidden, give, keep, pair, paired, own_part, arrive, joint,
     send, recv, z_send, local, tok_sem, swap_send, swap_recv, n2_send, n2_recv,
-    core_send, core_recv, pair_send, pair_recv, back_send, back_recv,
+    core_send, core_recv, pair_send, pair_recv, back_send, back_recv, joint_send,
 ):
     fs, tp = lax.axis_index("fs"), lax.axis_index("tp")
     z, p = fs // PLANE, fs % PLANE
@@ -233,10 +233,15 @@
     inner = ((z + 1) // 2) % 2
     layer = (z, z + 1 - 2 * (z % 2), 2 - z // 2, 3 - 3 * (z // 2))
     lands = (0, 1, 3 - inner, 3 - inner)
+    down = (
+        ((inner, 3 * (z // 2)), (2, layer[2])),
+        ((1 - inner, 1 + z // 2), (3, layer[3])),
+    )
     line = [(zz * PLANE + p, tp) for zz in layer]
     x_target, y_target = (z * PLANE + px, tp), (z * PLANE + py, tp)
     core_target = (fs, 1 - tp)
-    greet(line[1:] + [x_target, y_target, core_target])
+    with jax.named_scope("greet"):
+        greet(line[1:] + [x_target, y_target, core_target])
 
     rows, half = tok.shape
     deep, local_width = rb.shape
@@ -270,36 +275,39 @@
     def z_hop(a, source, f, slot, land, to):
         return hop(source, arrays[a][0](f), z_send.at[a, slot], recv.at[a, 0, land], line[to])
 
-    def sides(a, k):
+    def sides(a, k, of=None):
         at = arrays[a][0]
-        f = layer[k] * PLANE + p
-        source = piece(a, z) if k == 0 else at(f)
+        f = (layer[k] if of is None else of) * PLANE + p
+        source = piece(a, z) if of is None and k == 0 else at(f)
         for kind, target in ((1, x_target), (2, y_target)):
             c = hop(source, at(f), send.at[a, kind, k], recv.at[a, kind, k], target)
             c.start()
             pending.append(c)
 
-    def corners(a, k):
+    def corners(a, k, of=None):
         at = arrays[a][0]
-        base = layer[k] * PLANE
+        base = (layer[k] if of is None else of) * PLANE
         for kind, part, owner, target in ((1, 0, px, y_target), (2, 1, py, x_target)):
             whole = at(base + owner)
-            hop(whole, whole, send.at[a, kind, k], recv.at[a, kind, k], target).wait_recv()
+            with jax.named_scope(f"side{a}{k if of is None else 9}{kind}"):
+                hop(whole, whole, send.at[a, kind, k], recv.at[a, kind, k], target).wait_recv()
             block = at(base + owner, part)
             c = hop(block, block, send.at[a, kind + 2, k], recv.at[a, kind + 2, k], target)
             c.start()
             pending.append(c)
 
-    def corners_done(a, k):
+    def corners_done(a, k, of=None):
         at = arrays[a][0]
-        corner = layer[k] * PLANE + (PLANE - 1 - p)
+        corner = (layer[k] if of is None else of) * PLANE + (PLANE - 1 - p)
         for kind, part, target in ((1, 0, y_target), (2, 1, x_target)):
             block = at(corner, part)
-            hop(block, block, send.at[a, kind + 2, k], recv.at[a, kind + 2, k], target).wait_recv()
+            with jax.named_scope(f"corner{a}{k if of is None else 9}{kind}"):
+                hop(block, block, send.at[a, kind + 2, k], recv.at[a, kind + 2, k], target).wait_recv()
 
     def z_done(a, k):
         block = arrays[a][0](layer[k] * PLANE + p)
-        hop(block, block, z_send.at[a, 0], recv.at[a, 0, k], line[k]).wait_recv()
+        with jax.named_scope(f"z{a}{k}"):
+            hop(block, block, z_send.at[a, 0], recv.at[a, 0, k], line[k]).wait_recv()
 
     @pl.when(inner == 1)
     def _():
@@ -368,29 +376,36 @@
 
         inner_pending.extend((a, slot) for a in range(N_SMALL))
 
+    def ffn_along_z(where):
+        @pl.when(inner == where)
+        def _():
+            for a in range(N_SMALL, N_BIG):
+                for k in range(1, LAYERS):
+                    z_hop(a, piece(a, layer[k]), fs, k, lands[k], k).start()
+
     for k, to, land in ((1, 2, 3), (2, 1, 2), (3, 1, 3)):
         for a in range(N_SMALL):
             z_done(a, k)
         relay(k, to, land, k + 1)
+        if k > 1:
+            ffn_along_z(k - 2)
         for a in range(N_SMALL):
             sides(a, k)
+        if k == 2:
+            for a in range(N_SMALL):
+                corners(a, 0)
+    for k in range(1, LAYERS):
         for a in range(N_SMALL):
-            corners(a, k - 1)
-    for a in range(N_SMALL, N_BIG):
-        for k in range(1, LAYERS):
-            c = z_hop(a, piece(a, layer[k]), fs, k, lands[k], k)
-            c.start()
-            pending.append(c)
-    for a in range(N_SMALL):
-        corners(a, LAYERS - 1)
+            corners(a, k)
     sides(3, 0)
     z_done(3, 1)
     sides(3, 1)
 
-    tok_copy.wait_recv()
-    own[2].wait()
+    with jax.named_scope("tokens"):
+        tok_copy.wait_recv()
+        own[2].wait()
     wide_tok = whole_tok[...].astype(F32)
-    normed[...] = normed_rows(wide_tok, gain1[...].astype(F32))
+    normed[...] = normed_rows(wide_tok, gain1[...].astype(F32)[None, :])
     for c in own[3:]:
         c.wait()
     for k in range(LAYERS):
@@ -422,9 +437,8 @@
         mixed[:, at] = (d * gelu(outgate)).astype(BF16)
         return 0
 
-    lax.fori_loop(0, local_width // cw, mixer_chunk, 0)
-    z_done(3, 2)
-    sides(3, 2)
+    with jax.named_scope("mixer"):
+        lax.fori_loop(0, local_width // cw, mixer_chunk, 0)
     mix_wide = mine.shape[2]
     swaps = []
     for c in range(mine.shape[0]):
@@ -434,19 +448,18 @@
         s = hop(mine.at[c], theirs.at[c], swap_send.at[c], swap_recv.at[c], core_target)
         s.start()
         swaps.append(s)
-    z_done(3, 3)
-    sides(3, 3)
     square = jnp.zeros((rows, 1), F32)
     for c in range(mine.shape[0]):
         at = slice(c * mix_wide, (c + 1) * mix_wide)
-        swaps[c].wait_recv()
+        with jax.named_scope(f"swap{c}"):
+            swaps[c].wait_recv()
         both = mine[c].astype(F32) + theirs[c].astype(F32)
         total = (whole_tok[:, at].astype(F32) + both).astype(BF16)
         after[:, at] = total
         total = total.astype(F32)
         square = square + jnp.sum(total * total, axis=-1, keepdims=True)
     factor = lax.rsqrt(square * (1.0 / after.shape[1]) + EPS)
-    n2[0] = (after[...].astype(F32) * factor * gain2[...].astype(F32)).astype(BF16)
+    n2[0] = (after[...].astype(F32) * factor * gain2[...].astype(F32)[None, :]).astype(BF16)
 
     mine_half = span(tp, half)
 
@@ -462,28 +475,39 @@
     c = rows_hop(0, 1, 0, 1)
     c.start()
     pending.append(c)
-    across = {}
 
     def rows_arrived(k, to, land):
-        rows_hop(k, k, 0, 1).wait_recv()
+        with jax.named_scope(f"rows{k}"):
+            rows_hop(k, k, 0, 1).wait_recv()
 
         @pl.when(inner == 1)
         def _():
             rows_hop(k, land, k + 1, to).start()
 
+        core_hop(k).start()
+
+    def core_hop(k):
         block = n2.at[k, :, mine_half]
-        across[k] = hop(block, block, core_send.at[k], core_recv.at[k], core_target)
-        across[k].start()
-
-    for k in range(LAYERS):
-        corners(3, k)
-    dn_order = (0, 2, 1, 3)
-    sides(4, 0)
-    for k in dn_order[1:]:
-        z_done(4, k)
-        sides(4, k)
+        return hop(block, block, core_send.at[k], core_recv.at[k], core_target)
+
+    for k in (2, 3):
+        z_done(3, k)
+        sides(3, k)
+    corners(3, 0)
+    corners(3, 1)
     rows_arrived(1, 2, 3)
+    corners(3, 2)
     rows_arrived(2, 1, 2)
+    corners(3, 3)
+    z_done(4, 1)
+    z_done(4, 2)
+    down_a, down_b = down[0]
+    sides(4, *down_a)
+    sides(4, *down_b)
+
+    @pl.when(inner == 1)
+    def _():
+        rows_arrived(3, 1, 3)
 
     def up(k):
         place = position((rows, 4 * LANES))
@@ -507,32 +531,42 @@
             hidden[k, :, full * LANES : (full + 1) * LANES] = jnp.where(lane < rest, h, 0.0).astype(BF16)
 
     def up_step(k, _):
-        up(k)
+        with jax.named_scope("up"):
+            up(k)
         return 0
 
     for k in range(LAYERS):
         corners_done(3, k)
     lax.fori_loop(0, 1, up_step, 0)
-    corners(4, 0)
-    corners(4, 2)
-    across[1].wait_recv()
-    across[2].wait_recv()
-    rows_arrived(3, 1, 3)
-    lax.fori_loop(1, 3, up_step, 0)
-    corners(4, 1)
-    corners(4, 3)
-    across[3].wait_recv()
+    with jax.named_scope("across12"):
+        core_hop(1).wait_recv()
+        core_hop(2).wait_recv()
+    lax.fori_loop(1, 2, up_step, 0)
+    corners(4, *down_a)
+    lax.fori_loop(2, 3, up_step, 0)
+    corners(4, *down_b)
+    z_done(4, 3)
+    for block in down[1]:
+        sides(4, *block)
+
+    @pl.when(inner == 0)
+    def _():
+        rows_arrived(3, 1, 3)
+
+    with jax.named_scope("across3"):
+        core_hop(3).wait_recv()
     lax.fori_loop(3, 4, up_step, 0)
 
     turn = (tp + z // 2) % 2
     chunk = PLANE * wide
-    backs = []
-    for i in range(LAYERS // 2):
-        first, second = layer[i], layer[i + 2]
+    step_count = LAYERS // 2
+
+    def chunk_sum(i):
+        first, second = down[i][0][1], down[i][1][1]
         kept = first * (1 - turn) + second * turn
         given = first * turn + second * (1 - turn)
-        corners_done(4, i)
-        corners_done(4, i + 2)
+        for block in down[i]:
+            corners_done(4, *block)
 
         def give_step(k, _):
             give[i, k] = jnp.dot(
@@ -551,34 +585,71 @@
         s.start()
         pending.append(s)
         lax.fori_loop(0, LAYERS, keep_step, 0)
-        s.wait_recv()
-        place_at = span(kept % 2, chunk)
+        with jax.named_scope(f"pair{i}"):
+            s.wait_recv()
 
         def pair_step(k, _):
             paired[i, k] = (keep[k].astype(F32) + pair[i, k].astype(F32)).astype(BF16)
             return 0
 
         lax.fori_loop(0, LAYERS, pair_step, 0)
-        own_part[:, place_at] = paired[i, 0]
+        return span(kept % 2, chunk)
+
+    def to_partner(i, k, place):
+        landing = arrive.at[0, :, place] if k == 1 else joint.at[i, k - 2]
+        return hop(paired.at[i, k], landing, back_send.at[i, k], back_recv.at[i, k], line[1])
+
+    def to_layer(i, k, place):
+        return hop(joint.at[i, k], arrive.at[1, :, place], joint_send.at[i, k], back_recv.at[i, 0], line[k + 2])
+
+    places = []
+    for i in range(step_count):
+        place = chunk_sum(i)
+        places.append(place)
+        own_part[:, place] = paired[i, 0]
+
+        @pl.when(inner == 0)
+        def _():
+            for k in (2, 3):
+                to_partner(i, k, place).start()
+
+        to_partner(i, 1, place).start()
+        if i == 0:
+            for block in down[1]:
+                corners(4, *block)
+    for i in range(step_count):
+        place = places[i]
+
+        @pl.when(inner == 1)
+        def _():
+            for k in range(2):
+                with jax.named_scope(f"joint{i}{k}"):
+                    to_partner(i, k + 2, place).wait_recv()
+                joint[i, k] = (joint[i, k].astype(F32) + paired[i, k + 2].astype(F32)).astype(BF16)
+                to_layer(i, k, place).start()
+
+    for i in range(step_count):
+        with jax.named_scope(f"near{i}"):
+            to_partner(i, 1, places[i]).wait_recv()
+    for i in range(step_count):
+        with jax.named_scope(f"far{i}"):
+            to_layer(i, 0, places[i]).wait_recv()
+    total = own_part[...].astype(F32) + arrive[0].astype(F32) + arrive[1].astype(F32)
+    out[...] = (after[:, mine_half].astype(F32) + total).astype(BF16)
+
+    for c in pending + swaps + [core_hop(k) for k in range(1, LAYERS)] + [tok_copy]:
+        c.wait_send()
+    for a in range(N_SMALL, N_BIG):
         for k in range(1, LAYERS):
-            c = hop(
-                paired.at[i, k], arrive.at[lands[k] - 1, :, place_at],
-                back_send.at[i, k], back_recv.at[i, lands[k]], line[k],
-            )
-            c.start()
-            pending.append(c)
-            block = arrive.at[k - 1, :, place_at]
-            backs.append(hop(paired.at[i, k], block, back_send.at[i, k], back_recv.at[i, k], line[k]))
-
-    for c in backs:
-        c.wait_recv()
-    total = own_part[...].astype(F32)
-    for k in range(LAYERS - 1):
-        total = total + arrive[k].astype(F32)
-    out[...] = (after[:, mine_half].astype(F32) + total).astype(BF16)
-
-    for c in pending + swaps + list(across.values()) + [tok_copy]:
-        c.wait_send()
+            z_hop(a, piece(a, z), fs, k, 1, k).wait_send()
+    for i in range(step_count):
+        to_partner(i, 1, places[i]).wait_send()
+
+    @pl.when(inner == 0)
+    def _():
+        for i in range(step_count):
+            for k in (2, 3):
+                to_partner(i, k, places[i]).wait_send()
 
     @pl.when(inner == 1)
     def _():
@@ -586,6 +657,9 @@
             z_hop(a, arrays[a][0](fs), fs, slot, 0, 1).wait_send()
         for slot in range(1, LAYERS + 1):
             rows_hop(0, 0, slot, 1).wait_send()
+        for i in range(step_count):
+            for k in range(2):
+                to_layer(i, k, places[i]).wait_send()
 
 
 def fused_layer(
@@ -642,7 +716,8 @@
         pltpu.VMEM((2, LAYERS, rows, chunk), BF16),
         pltpu.VMEM((2, LAYERS, rows, chunk), BF16),
         pltpu.VMEM((rows, half), BF16),
-        pltpu.VMEM((LAYERS - 1, rows, half), BF16),
+        pltpu.VMEM((2, rows, half), BF16),
+        pltpu.VMEM((2, 2, rows, chunk), BF16),
         dma((N_BIG, 5, LAYERS)),
         dma((N_BIG, 5, LAYERS)),
         dma((N_BIG, LAYERS + 1)),
@@ -658,6 +733,7 @@
         dma((2,)),
         dma((2, LAYERS)),
         dma((2, LAYERS)),
+        dma((2, 2)),
     ]
     return pl.pallas_call(
         layer_kernel,
@@ -671,7 +747,7 @@
         name="layer",
     )(
         tokens,
-        mixer_norm_gain.reshape(1, -1),
+        mixer_norm_gain,
         recurrence_branch_weight,
         output_gate_projection,
         recurrence_conv_taps,
@@ -680,7 +756,7 @@
         channel_decay_rate.reshape(1, -1),
         position_log_decay,
         mixer_output_weight,
-        feedforward_norm_gain.reshape(1, -1),
+        feedforward_norm_gain,
         gate_up_weight,
         value_up_weight,
         gate_conv_taps,

time: 185 us -> 168 us (0.908)
  Pallas kernels: 181 us -> 166 us
  local copies, waits for them, and re-layouts: 3.77 us -> 1.87 us
    pallas_call x1, Pallas kernels: 181 us -> 166 us  [fused_layer(): pl.pallas_call(layer_kernel, out_shape=jax.ShapeDtypeStruct((rows, half),...]
    reshape x2 -> x0, local copies, waits for them, and re-layouts: 1.9 us -> none  [the longest x1 1.3 us: fused_layer(): mixer_norm_gain.reshape(1, -1)]
where the time goes in v1:
time: 168 us
  Pallas kernels  166 us (99%)
  local copies, waits for them, and re-layouts  1.87 us (1%)
    pallas_call x1, Pallas kernels, fused_layer(): pl.pallas_call(layer_kernel, out_shape=jax.ShapeDtypeStruct((rows, half),...  166 us

profile of v1, /device:TPU:0, one launch (start us, length us, event | category | flops | bytes accessed | tf_op | source)
XLA Modules:
  0.0 168.3 jit_solution(4812609768957380456)
XLA Ops:
  0.0 166.4 %layer.1 = bf16[256,1024]{1,0:T(8,128)(2,1)} custom-call(bf16[256,1024]{1,0:T(8,128)(2,1)} %tok.1, bf16[2048]{0:T(1024)(128)(2,1)} %gain1.1, bf16[128,512]{1,0:T(8,128)(2,1)} %rb.1, bf16[128,512]{1,0:T(8,128)(2,1)} %og.1, bf16[4,512]{1,0:T(4,128)(2,1)} %ctaps.1, bf16[8,64,64]{2,1,0:T(8,128)(2,1)} %rmap.1, bf16[8,64,64]{2,1,0:T(8,128)(2,1)} %imap.1, ...), custom_call_target="tpu_custom_call" | custom-call | tf_op jit(solution)/shard_map/layer/pallas_call | solution.py:738
  166.4 1.9 %copy.18 = bf16[256,1024]{1,0:T(8,128)(2,1)} copy(bf16[256,1024]{1,0:T(8,128)(2,1)} %layer.1) | data formatting | bytes 1048576

commit v2 on v1

--- a/solution.py
+++ b/solution.py
@@ -170,19 +170,23 @@
 
 
 def row_blocks(whole, deep, columns):
+    cut = deep * 3 // 4 // 16 * 16
+
     def at(f, part=None):
         if part is None:
             return whole.at[span(f, deep), columns]
-        return whole.at[span(f * 2 + part, deep // 2), columns]
+        start, size = ((0, cut), (cut, deep - cut))[part]
+        return whole.at[pl.ds(pl.multiple_of(f * deep + start, 16), size), columns]
 
     return at
 
 
 def column_blocks(whole, rows, wide):
+    cut = rows // 2 // 16 * 16
+
     def at(f, part=None):
-        if part is None:
-            return whole.at[pl.ds(0, rows), span(f, wide)]
-        return whole.at[pl.ds(part * (rows // 2), rows // 2), span(f, wide)]
+        start, size = ((0, rows) if part is None else ((0, cut), (cut, rows - cut))[part])
+        return whole.at[pl.ds(start, size), span(f, wide)]
 
     return at
 
@@ -221,9 +225,9 @@
 def layer_kernel(
     tok, gain1, rb, og, ctaps, rmap, imap, rate, pld, mo, gain2, gup, vup, gtaps, vtaps, dn,
     out,
-    whole_tok, bo_all, mo_all, gup_v, vup_v, stage, gu_all, dn_all, taps, gmap, pld_v,
-    normed, mixed, mine, theirs, after, n2, hidden, give, keep, pair, paired, own_part, arrive, joint,
-    send, recv, z_send, local, tok_sem, swap_send, swap_recv, n2_send, n2_recv,
+    tok2, bo_all, mo_all, gup_v, vup_v, stage, gu_all, dn_all, taps, gmap, pld_v,
+    normed, mix_give, mix_keep, mix_pair, mix_out, mix_in, after, n2, hidden, give, pair, paired, arrive, joint, out_v,
+    send, recv, z_send, local, misc, n2_send, n2_recv,
     core_send, core_recv, pair_send, pair_recv, back_send, back_recv, joint_send,
 ):
     fs, tp = lax.axis_index("fs"), lax.axis_index("tp")
@@ -234,8 +238,8 @@
     layer = (z, z + 1 - 2 * (z % 2), 2 - z // 2, 3 - 3 * (z // 2))
     lands = (0, 1, 3 - inner, 3 - inner)
     down = (
-        ((inner, 3 * (z // 2)), (2, layer[2])),
-        ((1 - inner, 1 + z // 2), (3, layer[3])),
+        ((1 - inner, 1 + z // 2), (2, layer[2])),
+        ((inner, 3 * (z // 2)), (3, layer[3])),
     )
     line = [(zz * PLANE + p, tp) for zz in layer]
     x_target, y_target = (z * PLANE + px, tp), (z * PLANE + py, tp)
@@ -249,6 +253,7 @@
     units = dn.shape[0] // LAYERS
     full, rest = units // LANES, units % LANES
     cw = gmap.shape[1]
+    mine_half, their_half, channels = span(tp, half), span(1 - tp, half), span(x, cw)
     heads, head = rmap.shape[:2]
     per = cw // head
 
@@ -268,9 +273,17 @@
     pending = []
     inner_pending = []
 
-    copy = hop(tok, whole_tok.at[:, span(tp, half)], tok_sem.at[0], tok_sem.at[1], core_target)
-    copy.start()
-    tok_copy = copy
+    def misc_hop(n, source, to, target):
+        return hop(source, to, misc.at[2 * n], misc.at[2 * n + 1], target)
+
+    def mixer_part(a, f, h):
+        if a < 2:
+            columns = pl.ds(pl.multiple_of(a * local_width + h * cw, cw), cw)
+            return bo_all.at[span(f, deep), columns]
+        return mo_all.at[span(h, cw), span(f, wide)]
+
+    def own_part_of(a, h):
+        return mo.at[span(h, cw), :] if a == 2 else arrays[a][1].at[:, span(h, cw)]
 
     def z_hop(a, source, f, slot, land, to):
         return hop(source, arrays[a][0](f), z_send.at[a, slot], recv.at[a, 0, land], line[to])
@@ -283,6 +296,30 @@
             c = hop(source, at(f), send.at[a, kind, k], recv.at[a, kind, k], target)
             c.start()
             pending.append(c)
+
+    def mixer_sides(a, k):
+        f = layer[k] * PLANE + p
+        for kind, h, target in ((1, 1 - x, x_target), (2, x, y_target)):
+            to = mixer_part(a, f, h)
+            c = hop(own_part_of(a, h) if k == 0 else to, to, send.at[a, kind, k], recv.at[a, kind, k], target)
+            c.start()
+            pending.append(c)
+
+    def mixer_hop(a, k, kind, owner, target):
+        block = mixer_part(a, layer[k] * PLANE + owner, x)
+        return hop(block, block, send.at[a, kind, k], recv.at[a, kind, k], target)
+
+    def mixer_corner(a, k):
+        with jax.named_scope(f"side{a}{k}"):
+            mixer_hop(a, k, 1, px, x_target).wait_recv()
+        c = mixer_hop(a, k, 3, px, y_target)
+        c.start()
+        pending.append(c)
+
+    def mixer_done(a, k):
+        with jax.named_scope(f"corner{a}{k}"):
+            mixer_hop(a, k, 2, py, y_target).wait_recv()
+            mixer_hop(a, k, 3, PLANE - 1 - p, y_target).wait_recv()
 
     def corners(a, k, of=None):
         at = arrays[a][0]
@@ -320,13 +357,19 @@
         pending.append(c)
     inner_pending += [(a, 1) for a in range(N_SMALL)]
     for a in range(N_SMALL):
-        sides(a, 0)
+        mixer_sides(a, 0)
+    tok_swap = misc_hop(0, tok, tok2.at[0, :, mine_half], core_target)
+    tok_x = misc_hop(1, tok, tok2.at[1, :, mine_half], x_target)
+    pld_x = misc_hop(2, pld.at[:, span(1 - x, cw)], pld_v.at[1], x_target)
+    tok_swap.start()
+    pld_x.start()
+    pending += [tok_swap, tok_x, pld_x]
 
     own = [
         pltpu.make_async_copy(gup, gup_v, local.at[0]),
         pltpu.make_async_copy(vup, vup_v, local.at[1]),
-        pltpu.make_async_copy(tok, whole_tok.at[:, span(tp, half)], local.at[2]),
-        pltpu.make_async_copy(pld, pld_v, local.at[3]),
+        pltpu.make_async_copy(tok, tok2.at[0, :, mine_half], local.at[2]),
+        pltpu.make_async_copy(pld.at[:, channels], pld_v.at[0], local.at[3]),
         pltpu.make_async_copy(rb, arrays[0][0](fs), local.at[4]),
         pltpu.make_async_copy(og, arrays[1][0](fs), local.at[5]),
         pltpu.make_async_copy(mo, arrays[2][0](fs), local.at[6]),
@@ -390,36 +433,45 @@
         if k > 1:
             ffn_along_z(k - 2)
         for a in range(N_SMALL):
-            sides(a, k)
-        if k == 2:
-            for a in range(N_SMALL):
-                corners(a, 0)
-    for k in range(1, LAYERS):
+            mixer_sides(a, k)
+        if k == 1:
+            tok_x.start()
         for a in range(N_SMALL):
-            corners(a, k)
+            mixer_corner(a, k - 1)
+    with jax.named_scope("tok_x"):
+        tok_x.wait_recv()
+    block = tok2.at[1, :, mine_half]
+    tok_core = misc_hop(3, block, block, core_target)
+    tok_core.start()
+    pending.append(tok_core)
+    for a in range(N_SMALL):
+        mixer_corner(a, LAYERS - 1)
     sides(3, 0)
-    z_done(3, 1)
-    sides(3, 1)
 
     with jax.named_scope("tokens"):
-        tok_copy.wait_recv()
+        tok_swap.wait_recv()
+        tok_core.wait_recv()
+        pld_x.wait_recv()
         own[2].wait()
-    wide_tok = whole_tok[...].astype(F32)
-    normed[...] = normed_rows(wide_tok, gain1[...].astype(F32)[None, :])
+
+    def norm_step(r, _):
+        normed[r] = normed_rows(tok2[r].astype(F32), gain1[...].astype(F32)[None, :])
+        return 0
+
+    lax.fori_loop(0, 2, norm_step, 0)
     for c in own[3:]:
         c.wait()
     for k in range(LAYERS):
         for a in range(N_SMALL):
-            corners_done(a, k)
-
-    def mixer_chunk(c, _):
-        at = span(c, cw)
+            mixer_done(a, k)
+
+    def mixer_rows(r, _):
         place = position((rows, cw))
-        branch = jnp.dot(normed[...], bo_all[:, at], preferred_element_type=F32)
+        branch = jnp.dot(normed[r], bo_all[:, channels], preferred_element_type=F32)
         branch = branch.astype(BF16).astype(F32)
-        conv = rows_conv(branch, ctaps[:, at].astype(F32), ctaps.shape[0], place).astype(BF16)
-        gates = jax.nn.sigmoid(jnp.dot(conv, gmap[c], preferred_element_type=F32))
-        la = -DECAY_RATE_GAIN * gates[:, :cw] * rate[:, at] + pld_v[:, at]
+        conv = rows_conv(branch, ctaps[:, channels].astype(F32), ctaps.shape[0], place).astype(BF16)
+        gates = jax.nn.sigmoid(jnp.dot(conv, gmap[x], preferred_element_type=F32))
+        la = -DECAY_RATE_GAIN * gates[:, :cw] * rate[:, channels] + pld_v[r]
         d = jnp.sqrt(negative_expm1(2.0 * la)) * gates[:, cw:] * conv.astype(F32)
         a = jnp.exp(la)
         step = 1
@@ -429,39 +481,47 @@
                 a = a * shifted(a, step, place, 1.0)
             step *= 2
         outgate = jnp.dot(
-            normed[...],
-            bo_all[:, pl.ds(pl.multiple_of(local_width + c * cw, cw), cw)],
+            normed[r],
+            bo_all[:, pl.ds(pl.multiple_of(local_width + x * cw, cw), cw)],
             preferred_element_type=F32,
         )
         outgate = outgate.astype(BF16).astype(F32)
-        mixed[:, at] = (d * gelu(outgate)).astype(BF16)
+        mixed = (d * gelu(outgate)).astype(BF16)
+        mix_give[r] = jnp.dot(mixed, mo_all[channels, their_half], preferred_element_type=F32).astype(BF16)
+        mix_keep[r] = jnp.dot(mixed, mo_all[channels, mine_half], preferred_element_type=F32)
         return 0
 
-    with jax.named_scope("mixer"):
-        lax.fori_loop(0, local_width // cw, mixer_chunk, 0)
-    mix_wide = mine.shape[2]
-    swaps = []
-    for c in range(mine.shape[0]):
-        mine[c] = jnp.dot(
-            mixed[...], mo_all[:, c * mix_wide : (c + 1) * mix_wide], preferred_element_type=F32
-        ).astype(BF16)
-        s = hop(mine.at[c], theirs.at[c], swap_send.at[c], swap_recv.at[c], core_target)
-        s.start()
-        swaps.append(s)
-    square = jnp.zeros((rows, 1), F32)
-    for c in range(mine.shape[0]):
-        at = slice(c * mix_wide, (c + 1) * mix_wide)
-        with jax.named_scope(f"swap{c}"):
-            swaps[c].wait_recv()
-        both = mine[c].astype(F32) + theirs[c].astype(F32)
-        total = (whole_tok[:, at].astype(F32) + both).astype(BF16)
-        after[:, at] = total
-        total = total.astype(F32)
-        square = square + jnp.sum(total * total, axis=-1, keepdims=True)
-    factor = lax.rsqrt(square * (1.0 / after.shape[1]) + EPS)
-    n2[0] = (after[...].astype(F32) * factor * gain2[...].astype(F32)[None, :]).astype(BF16)
-
-    mine_half = span(tp, half)
+    def mix_hop(r):
+        return misc_hop(4 + r, mix_give.at[r], mix_pair.at[r], core_target)
+
+    with jax.named_scope("mixer1"):
+        lax.fori_loop(1, 2, mixer_rows, 0)
+    mix_hop(1).start()
+    with jax.named_scope("mixer0"):
+        lax.fori_loop(0, 1, mixer_rows, 0)
+    mix_hop(0).start()
+    with jax.named_scope("swap1"):
+        mix_hop(1).wait_recv()
+    mix_out[...] = (mix_keep[1] + mix_pair[1].astype(F32)).astype(BF16)
+    mix_x = misc_hop(6, mix_out, mix_in, x_target)
+    mix_x.start()
+    for k in range(1, LAYERS):
+        z_done(3, k)
+        sides(3, k)
+    with jax.named_scope("swap0"):
+        mix_hop(0).wait_recv()
+    mix_keep[0] = mix_keep[0] + mix_pair[0].astype(F32) + tok2[0, :, mine_half].astype(F32)
+    with jax.named_scope("mix_x"):
+        mix_x.wait_recv()
+    after[:, mine_half] = (mix_keep[0] + mix_in[...].astype(F32)).astype(BF16)
+    after_core = misc_hop(7, after.at[:, mine_half], after.at[:, mine_half], core_target)
+    after_core.start()
+    pending += [mix_hop(0), mix_hop(1), mix_x, after_core]
+    corners(3, 0)
+    with jax.named_scope("after"):
+        after_core.wait_recv()
+    n2[0] = normed_rows(after[...].astype(F32), gain2[...].astype(F32)[None, :])
+
 
     def rows_hop(k, land, slot, to):
         return hop(
@@ -490,10 +550,6 @@
         block = n2.at[k, :, mine_half]
         return hop(block, block, core_send.at[k], core_recv.at[k], core_target)
 
-    for k in (2, 3):
-        z_done(3, k)
-        sides(3, k)
-    corners(3, 0)
     corners(3, 1)
     rows_arrived(1, 2, 3)
     corners(3, 2)
@@ -502,12 +558,13 @@
     z_done(4, 1)
     z_done(4, 2)
     down_a, down_b = down[0]
-    sides(4, *down_a)
-    sides(4, *down_b)
 
     @pl.when(inner == 1)
     def _():
         rows_arrived(3, 1, 3)
+
+    sides(4, *down_a)
+    sides(4, *down_b)
 
     def up(k):
         place = position((rows, 4 * LANES))
@@ -535,19 +592,70 @@
             up(k)
         return 0
 
+    turn = (tp + z // 2) % 2
+    quarter = PLANE * wide // 2
+
+    def columns_of(j, mine):
+        first, second = down[j // 2][0][1], down[j // 2][1][1]
+        side = turn if mine else 1 - turn
+        block = first * (1 - side) + second * side
+        return block * 2 + (y if j % 2 == 0 else 1 - y)
+
+    def place_of(j):
+        return columns_of(j, True) % (half // quarter)
+
+    def pair_hop(j, k):
+        return hop(give.at[j, k], pair.at[j, k], pair_send.at[j, k], pair_recv.at[j, k], core_target)
+
+    def to_partner(j, k):
+        landing = arrive.at[0, j] if k == 1 else joint.at[j, k - 2]
+        return hop(paired.at[j, k], landing, back_send.at[j, k], back_recv.at[j, k], line[1])
+
+    def to_layer(j, k):
+        return hop(joint.at[j, k], arrive.at[1, j], joint_send.at[j, k], back_recv.at[j, 0], line[k + 2])
+
+    def part_sums(j, slots):
+        given, kept = span(columns_of(j, False), quarter), span(columns_of(j, True), quarter)
+        for k in slots:
+            give[j, k] = jnp.dot(hidden[k], dn_all[:, given], preferred_element_type=F32).astype(BF16)
+            pair_hop(j, k).start()
+        for k in slots:
+            keep = jnp.dot(hidden[k], dn_all[:, kept], preferred_element_type=F32)
+            with jax.named_scope(f"pair{j}{k}"):
+                pair_hop(j, k).wait_recv()
+            paired[j, k] = (keep + pair[j, k].astype(F32)).astype(BF16)
+            if k > 1:
+
+                @pl.when(inner == 0)
+                def _():
+                    to_partner(j, k).start()
+
+            elif k == 1:
+                to_partner(j, 1).start()
+
+    def joint_sums(j, k):
+        @pl.when(inner == 1)
+        def _():
+            with jax.named_scope(f"joint{j}{k}"):
+                to_partner(j, k + 2).wait_recv()
+            joint[j, k] = (joint[j, k].astype(F32) + paired[j, k + 2].astype(F32)).astype(BF16)
+            to_layer(j, k).start()
+
     for k in range(LAYERS):
         corners_done(3, k)
-    lax.fori_loop(0, 1, up_step, 0)
     with jax.named_scope("across12"):
         core_hop(1).wait_recv()
         core_hop(2).wait_recv()
-    lax.fori_loop(1, 2, up_step, 0)
+    lax.fori_loop(1, 3, up_step, 0)
     corners(4, *down_a)
-    lax.fori_loop(2, 3, up_step, 0)
     corners(4, *down_b)
     z_done(4, 3)
     for block in down[1]:
         sides(4, *block)
+    part_sums(0, (2, 1))
+    for block in down[0]:
+        corners_done(4, *block)
+    part_sums(1, (2, 1))
 
     @pl.when(inner == 0)
     def _():
@@ -556,100 +664,52 @@
     with jax.named_scope("across3"):
         core_hop(3).wait_recv()
     lax.fori_loop(3, 4, up_step, 0)
-
-    turn = (tp + z // 2) % 2
-    chunk = PLANE * wide
-    step_count = LAYERS // 2
-
-    def chunk_sum(i):
-        first, second = down[i][0][1], down[i][1][1]
-        kept = first * (1 - turn) + second * turn
-        given = first * turn + second * (1 - turn)
-        for block in down[i]:
-            corners_done(4, *block)
-
-        def give_step(k, _):
-            give[i, k] = jnp.dot(
-                hidden[k], dn_all[:, span(given, chunk)], preferred_element_type=F32
-            ).astype(BF16)
-            return 0
-
-        def keep_step(k, _):
-            keep[k] = jnp.dot(
-                hidden[k], dn_all[:, span(kept, chunk)], preferred_element_type=F32
-            ).astype(BF16)
-            return 0
-
-        lax.fori_loop(0, LAYERS, give_step, 0)
-        s = hop(give.at[i], pair.at[i], pair_send.at[i], pair_recv.at[i], core_target)
-        s.start()
-        pending.append(s)
-        lax.fori_loop(0, LAYERS, keep_step, 0)
-        with jax.named_scope(f"pair{i}"):
-            s.wait_recv()
-
-        def pair_step(k, _):
-            paired[i, k] = (keep[k].astype(F32) + pair[i, k].astype(F32)).astype(BF16)
-            return 0
-
-        lax.fori_loop(0, LAYERS, pair_step, 0)
-        return span(kept % 2, chunk)
-
-    def to_partner(i, k, place):
-        landing = arrive.at[0, :, place] if k == 1 else joint.at[i, k - 2]
-        return hop(paired.at[i, k], landing, back_send.at[i, k], back_recv.at[i, k], line[1])
-
-    def to_layer(i, k, place):
-        return hop(joint.at[i, k], arrive.at[1, :, place], joint_send.at[i, k], back_recv.at[i, 0], line[k + 2])
-
-    places = []
-    for i in range(step_count):
-        place = chunk_sum(i)
-        places.append(place)
-        own_part[:, place] = paired[i, 0]
-
-        @pl.when(inner == 0)
-        def _():
-            for k in (2, 3):
-                to_partner(i, k, place).start()
-
-        to_partner(i, 1, place).start()
-        if i == 0:
-            for block in down[1]:
-                corners(4, *block)
-    for i in range(step_count):
-        place = places[i]
-
-        @pl.when(inner == 1)
-        def _():
-            for k in range(2):
-                with jax.named_scope(f"joint{i}{k}"):
-                    to_partner(i, k + 2, place).wait_recv()
-                joint[i, k] = (joint[i, k].astype(F32) + paired[i, k + 2].astype(F32)).astype(BF16)
-                to_layer(i, k, place).start()
-
-    for i in range(step_count):
-        with jax.named_scope(f"near{i}"):
-            to_partner(i, 1, places[i]).wait_recv()
-    for i in range(step_count):
-        with jax.named_scope(f"far{i}"):
-            to_layer(i, 0, places[i]).wait_recv()
-    total = own_part[...].astype(F32) + arrive[0].astype(F32) + arrive[1].astype(F32)
-    out[...] = (after[:, mine_half].astype(F32) + total).astype(BF16)
-
-    for c in pending + swaps + [core_hop(k) for k in range(1, LAYERS)] + [tok_copy]:
+    part_sums(0, (3,))
+    part_sums(1, (3,))
+    corners(4, *down[1][0])
+    joint_sums(0, 0)
+    lax.fori_loop(0, 1, up_step, 0)
+    corners(4, *down[1][1])
+    joint_sums(1, 0)
+    part_sums(2, (3, 2, 1))
+    joint_sums(0, 1)
+    for block in down[1]:
+        corners_done(4, *block)
+    part_sums(3, (3, 2, 1))
+    joint_sums(1, 1)
+    for j in range(LAYERS):
+        part_sums(j, (0,))
+    for j in (2, 3):
+        for k in (1, 0):
+            joint_sums(j, k)
+
+    stores = []
+    for j in range(LAYERS):
+        with jax.named_scope(f"near{j}"):
+            to_partner(j, 1).wait_recv()
+        with jax.named_scope(f"far{j}"):
+            to_layer(j, 0).wait_recv()
+        total = paired[j, 0].astype(F32) + arrive[0, j].astype(F32) + arrive[1, j].astype(F32)
+        first = pl.multiple_of(tp * half + place_of(j) * quarter, quarter)
+        out_v[j] = (after[:, pl.ds(first, quarter)].astype(F32) + total).astype(BF16)
+        stores.append(pltpu.make_async_copy(out_v.at[j], out.at[:, span(place_of(j), quarter)], local.at[j]))
+        stores[j].start()
+
+    for c in pending + [core_hop(k) for k in range(1, LAYERS)]:
         c.wait_send()
     for a in range(N_SMALL, N_BIG):
         for k in range(1, LAYERS):
             z_hop(a, piece(a, z), fs, k, 1, k).wait_send()
-    for i in range(step_count):
-        to_partner(i, 1, places[i]).wait_send()
+    for j in range(LAYERS):
+        to_partner(j, 1).wait_send()
+        for k in range(LAYERS):
+            pair_hop(j, k).wait_send()
 
     @pl.when(inner == 0)
     def _():
-        for i in range(step_count):
+        for j in range(LAYERS):
             for k in (2, 3):
-                to_partner(i, k, places[i]).wait_send()
+                to_partner(j, k).wait_send()
 
     @pl.when(inner == 1)
     def _():
@@ -657,9 +717,12 @@
             z_hop(a, arrays[a][0](fs), fs, slot, 0, 1).wait_send()
         for slot in range(1, LAYERS + 1):
             rows_hop(0, 0, slot, 1).wait_send()
-        for i in range(step_count):
+        for j in range(LAYERS):
             for k in range(2):
-                to_layer(i, k, places[i]).wait_send()
+                to_layer(j, k).wait_send()
+
+    for c in stores:
+        c.wait()
 
 
 def fused_layer(
@@ -688,12 +751,11 @@
     local_units = gate_up_weight.shape[1]
     units = local_units // LAYERS
     padded = -(-units // (2 * LANES)) * 2 * LANES
-    head = recurrence_gate_map.shape[1]
-    cw = min(local_width, 4 * head)
-    chunk = PLANE * wide
+    cw = local_width // 2
+    quarter = PLANE * wide // 2
     dma = pltpu.SemaphoreType.DMA
     scratch = [
-        pltpu.VMEM((rows, features), BF16),
+        pltpu.VMEM((2, rows, features), BF16),
         pltpu.VMEM((n_fs * deep, 2 * local_width), BF16),
         pltpu.VMEM((local_width, n_fs * wide), BF16),
         pltpu.VMEM((deep, local_units), BF16),
@@ -703,43 +765,42 @@
         pltpu.VMEM((padded, n_fs * wide), BF16),
         pltpu.VMEM((LAYERS, 8, 2 * units), F32),
         pltpu.VMEM((local_width // cw, cw, 2 * cw), BF16),
-        pltpu.VMEM((rows, local_width), F32),
-        pltpu.VMEM((rows, features), BF16),
-        pltpu.VMEM((rows, local_width), BF16),
-        pltpu.VMEM((LAYERS, rows, chunk), BF16),
-        pltpu.VMEM((LAYERS, rows, chunk), BF16),
+        pltpu.VMEM((2, rows, cw), F32),
+        pltpu.VMEM((2, rows, features), BF16),
+        pltpu.VMEM((2, rows, half), BF16),
+        pltpu.VMEM((2, rows, half), F32),
+        pltpu.VMEM((2, rows, half), BF16),
+        pltpu.VMEM((rows, half), BF16),
+        pltpu.VMEM((rows, half), BF16),
         pltpu.VMEM((rows, features), BF16),
         pltpu.VMEM((LAYERS, rows, features), BF16),
         pltpu.VMEM((LAYERS, rows, padded), BF16),
-        pltpu.VMEM((2, LAYERS, rows, chunk), BF16),
-        pltpu.VMEM((LAYERS, rows, chunk), BF16),
-        pltpu.VMEM((2, LAYERS, rows, chunk), BF16),
-        pltpu.VMEM((2, LAYERS, rows, chunk), BF16),
-        pltpu.VMEM((rows, half), BF16),
-        pltpu.VMEM((2, rows, half), BF16),
-        pltpu.VMEM((2, 2, rows, chunk), BF16),
+        pltpu.VMEM((LAYERS, LAYERS, rows, quarter), BF16),
+        pltpu.VMEM((LAYERS, LAYERS, rows, quarter), BF16),
+        pltpu.VMEM((LAYERS, LAYERS, rows, quarter), BF16),
+        pltpu.VMEM((2, LAYERS, rows, quarter), BF16),
+        pltpu.VMEM((LAYERS, 2, rows, quarter), BF16),
+        pltpu.VMEM((LAYERS, rows, quarter), BF16),
         dma((N_BIG, 5, LAYERS)),
         dma((N_BIG, 5, LAYERS)),
         dma((N_BIG, LAYERS + 1)),
         dma((8,)),
-        dma((2,)),
-        dma((LAYERS,)),
-        dma((LAYERS,)),
+        dma((16,)),
         dma((LAYERS + 1,)),
         dma((LAYERS,)),
         dma((LAYERS,)),
         dma((LAYERS,)),
-        dma((2,)),
-        dma((2,)),
-        dma((2, LAYERS)),
-        dma((2, LAYERS)),
-        dma((2, 2)),
+        dma((LAYERS, LAYERS)),
+        dma((LAYERS, LAYERS)),
+        dma((LAYERS, LAYERS)),
+        dma((LAYERS, LAYERS)),
+        dma((LAYERS, 2)),
     ]
     return pl.pallas_call(
         layer_kernel,
         out_shape=jax.ShapeDtypeStruct((rows, half), BF16),
         in_specs=[ANY, VMEM, ANY, ANY, VMEM, VMEM, VMEM, VMEM, ANY, ANY, VMEM, ANY, ANY, VMEM, VMEM, ANY],
-        out_specs=VMEM,
+        out_specs=ANY,
         scratch_shapes=scratch,
         compiler_params=pltpu.CompilerParams(
             collective_id=0, has_side_effects=True, vmem_limit_bytes=62 * 2**20

time: 168 us -> 158 us (0.940)
  Pallas kernels: 166 us -> 155 us
    pallas_call x1, Pallas kernels: 166 us -> 155 us  [fused_layer(): pl.pallas_call(layer_kernel, out_shape=jax.ShapeDtypeStruct((rows, half),...]
where the time goes in v2:
time: 158 us; the launch traced here: 157 us
  Pallas kernels  155 us (98%)
  local copies, waits for them, and re-layouts  1.87 us (1%)
    pallas_call x1, Pallas kernels, fused_layer(): pl.pallas_call(layer_kernel, out_shape=jax.ShapeDtypeStruct((rows, half),...  155 us

profile of v2, /device:TPU:0, one launch (start us, length us, event | category | flops | bytes accessed | tf_op | source)
XLA Modules:
  0.0 157.1 jit_solution(15174215165699406529)
XLA Ops:
  0.0 155.3 %layer.1 = bf16[256,1024]{1,0:T(8,128)(2,1)} custom-call(bf16[256,1024]{1,0:T(8,128)(2,1)} %tok.1, bf16[2048]{0:T(1024)(128)(2,1)} %gain1.1, bf16[128,512]{1,0:T(8,128)(2,1)} %rb.1, bf16[128,512]{1,0:T(8,128)(2,1)} %og.1, bf16[4,512]{1,0:T(4,128)(2,1)} %ctaps.1, bf16[8,64,64]{2,1,0:T(8,128)(2,1)} %rmap.1, bf16[8,64,64]{2,1,0:T(8,128)(2,1)} %imap.1, ...), custom_call_target="tpu_custom_call" | custom-call | tf_op jit(solution)/shard_map/layer/pallas_call | solution.py:799
  155.3 1.9 %copy.18 = bf16[256,1024]{1,0:T(8,128)(2,1)} copy(bf16[256,1024]{1,0:T(8,128)(2,1)} %layer.1) | data formatting | bytes 1048576

commit v3 on v2

--- a/solution.py
+++ b/solution.py
@@ -143,6 +143,19 @@
 VMEM = pl.BlockSpec(memory_space=pltpu.VMEM)
 F32, BF16 = jnp.float32, jnp.bfloat16
 N_SMALL, N_BIG = 3, 5
+ROWS_CUT = 6
+MISC_HALVES = 15
+N_SENT = 13
+AT_Z = 0
+AT_MIX = AT_Z + N_BIG * LAYERS
+AT_MIX_DONE = AT_MIX + N_SMALL * LAYERS
+AT_SIDE = AT_MIX_DONE + 2
+AT_CORNER = AT_SIDE + 2 * 2 * LAYERS
+AT_MISC = AT_CORNER + 2 * 2 * 2
+AT_ROWS = AT_MISC + 8
+AT_CORE = AT_ROWS + LAYERS
+AT_PAIR = AT_CORE + LAYERS
+AT_BACK = AT_PAIR + LAYERS * LAYERS
 
 
 def hop(src, dst, send, recv, target):
@@ -170,7 +183,7 @@
 
 
 def row_blocks(whole, deep, columns):
-    cut = deep * 3 // 4 // 16 * 16
+    cut = ROWS_CUT * deep // 8
 
     def at(f, part=None):
         if part is None:
@@ -226,9 +239,8 @@
     tok, gain1, rb, og, ctaps, rmap, imap, rate, pld, mo, gain2, gup, vup, gtaps, vtaps, dn,
     out,
     tok2, bo_all, mo_all, gup_v, vup_v, stage, gu_all, dn_all, taps, gmap, pld_v,
-    normed, mix_give, mix_keep, mix_pair, mix_out, mix_in, after, n2, hidden, give, pair, paired, arrive, joint, out_v,
-    send, recv, z_send, local, misc, n2_send, n2_recv,
-    core_send, core_recv, pair_send, pair_recv, back_send, back_recv, joint_send,
+    normed, mix_give, mix_keep, mix_pair, mix_out, mix_in, after, n2, hidden, give, pair, paired, arrive, joint, out_v, part,
+    sent, got, local,
 ):
     fs, tp = lax.axis_index("fs"), lax.axis_index("tp")
     z, p = fs // PLANE, fs % PLANE
@@ -270,11 +282,13 @@
             return arrays[a][1]
         return stage.at[zz] if a == 3 else dn.at[span(zz, units), :]
 
-    pending = []
-    inner_pending = []
+    MIX, UP, DOWN, MIX_Z, MIX_RELAY, UP_Z, DOWN_Z, ROWS, ROWS_RELAY, MISC, PAIR, NEAR, FAR = range(N_SENT)
 
     def misc_hop(n, source, to, target):
-        return hop(source, to, misc.at[2 * n], misc.at[2 * n + 1], target)
+        return hop(source, to, sent.at[MISC], got.at[AT_MISC + n], target)
+
+    def arrival(block, n):
+        return hop(block, block, sent.at[MISC], got.at[n], core_target)
 
     def mixer_part(a, f, h):
         if a < 2:
@@ -286,65 +300,71 @@
         return mo.at[span(h, cw), :] if a == 2 else arrays[a][1].at[:, span(h, cw)]
 
     def z_hop(a, source, f, slot, land, to):
-        return hop(source, arrays[a][0](f), z_send.at[a, slot], recv.at[a, 0, land], line[to])
-
-    def sides(a, k, of=None):
+        group = (UP_Z, DOWN_Z)[a - N_SMALL] if a >= N_SMALL else MIX_RELAY if slot else MIX_Z
+        return hop(source, arrays[a][0](f), sent.at[group], got.at[AT_Z + a * LAYERS + land], line[to])
+
+    def side_at(a, k, kind):
+        return AT_SIDE + ((a - N_SMALL) * 2 + kind - 1) * LAYERS + k
+
+    def corner_at(a, late, kind):
+        return AT_CORNER + ((a - N_SMALL) * 2 + late) * 2 + kind - 1
+
+    def sides(a, k, of=None, kinds=(1, 2)):
         at = arrays[a][0]
         f = (layer[k] if of is None else of) * PLANE + p
         source = piece(a, z) if of is None and k == 0 else at(f)
-        for kind, target in ((1, x_target), (2, y_target)):
-            c = hop(source, at(f), send.at[a, kind, k], recv.at[a, kind, k], target)
-            c.start()
-            pending.append(c)
+        for kind in kinds:
+            target = (x_target, y_target)[kind - 1]
+            hop(source, at(f), sent.at[UP + a - N_SMALL], got.at[side_at(a, k, kind)], target).start()
 
     def mixer_sides(a, k):
+        copies = []
         f = layer[k] * PLANE + p
         for kind, h, target in ((1, 1 - x, x_target), (2, x, y_target)):
             to = mixer_part(a, f, h)
-            c = hop(own_part_of(a, h) if k == 0 else to, to, send.at[a, kind, k], recv.at[a, kind, k], target)
-            c.start()
-            pending.append(c)
-
-    def mixer_hop(a, k, kind, owner, target):
-        block = mixer_part(a, layer[k] * PLANE + owner, x)
-        return hop(block, block, send.at[a, kind, k], recv.at[a, kind, k], target)
+            source = own_part_of(a, h) if k == 0 else to
+            n = AT_MIX + a * LAYERS + k if kind == 1 else AT_MIX_DONE
+            copies.append(hop(source, to, sent.at[MIX], got.at[n], target))
+        return copies
 
     def mixer_corner(a, k):
+        block = mixer_part(a, layer[k] * PLANE + px, x)
         with jax.named_scope(f"side{a}{k}"):
-            mixer_hop(a, k, 1, px, x_target).wait_recv()
-        c = mixer_hop(a, k, 3, px, y_target)
-        c.start()
-        pending.append(c)
-
-    def mixer_done(a, k):
-        with jax.named_scope(f"corner{a}{k}"):
-            mixer_hop(a, k, 2, py, y_target).wait_recv()
-            mixer_hop(a, k, 3, PLANE - 1 - p, y_target).wait_recv()
-
-    def corners(a, k, of=None):
+            arrival(block, AT_MIX + a * LAYERS + k).wait_recv()
+        hop(block, block, sent.at[MIX], got.at[AT_MIX_DONE + 1], y_target).start()
+
+    def mixer_done():
+        block = bo_all.at[pl.ds(0, N_SMALL * LAYERS * deep // 4), :]
+        for n in range(2):
+            with jax.named_scope(f"mixer_done{n}"):
+                arrival(block, AT_MIX_DONE + n).wait_recv()
+
+    def corners(a, k, of=None, kinds=(1, 2)):
         at = arrays[a][0]
         base = (layer[k] if of is None else of) * PLANE
+        late = k == LAYERS - 1 if a == N_SMALL else of is down[1][0][1] or of is down[1][1][1]
         for kind, part, owner, target in ((1, 0, px, y_target), (2, 1, py, x_target)):
-            whole = at(base + owner)
+            if kind not in kinds:
+                continue
             with jax.named_scope(f"side{a}{k if of is None else 9}{kind}"):
-                hop(whole, whole, send.at[a, kind, k], recv.at[a, kind, k], target).wait_recv()
+                arrival(at(base + owner), side_at(a, k, kind)).wait_recv()
             block = at(base + owner, part)
-            c = hop(block, block, send.at[a, kind + 2, k], recv.at[a, kind + 2, k], target)
-            c.start()
-            pending.append(c)
-
-    def corners_done(a, k, of=None):
-        at = arrays[a][0]
-        corner = (layer[k] if of is None else of) * PLANE + (PLANE - 1 - p)
-        for kind, part, target in ((1, 0, y_target), (2, 1, x_target)):
-            block = at(corner, part)
-            with jax.named_scope(f"corner{a}{k if of is None else 9}{kind}"):
-                hop(block, block, send.at[a, kind + 2, k], recv.at[a, kind + 2, k], target).wait_recv()
+            hop(block, block, sent.at[UP + a - N_SMALL], got.at[corner_at(a, late, kind)], target).start()
+
+    def corners_done(a, late):
+        count = (1 if late else LAYERS - 1) if a == N_SMALL else 2
+        for kind in (1, 2):
+            if a == N_SMALL:
+                block = gu_all.at[pl.ds(0, count * (ROWS_CUT * deep // 8 if kind == 1 else deep - ROWS_CUT * deep // 8)), :]
+            else:
+                block = dn_all.at[pl.ds(0, units // 2), pl.ds(0, count * wide)]
+            with jax.named_scope(f"corner{a}{int(late)}{kind}"):
+                arrival(block, corner_at(a, late, kind)).wait_recv()
 
     def z_done(a, k):
         block = arrays[a][0](layer[k] * PLANE + p)
         with jax.named_scope(f"z{a}{k}"):
-            hop(block, block, z_send.at[a, 0], recv.at[a, 0, k], line[k]).wait_recv()
+            arrival(block, AT_Z + a * LAYERS + k).wait_recv()
 
     @pl.when(inner == 1)
     def _():
@@ -352,18 +372,21 @@
             z_hop(a, piece(a, z), fs, 1, 2, 2).start()
 
     for a in range(N_SMALL):
-        c = z_hop(a, piece(a, z), fs, 0, 1, 1)
+        z_hop(a, piece(a, z), fs, 0, 1, 1).start()
+    mixer_copies = [[c for a in range(N_SMALL) for c in mixer_sides(a, k)] for k in range(LAYERS)]
+    for c in mixer_copies[0]:
         c.start()
-        pending.append(c)
-    inner_pending += [(a, 1) for a in range(N_SMALL)]
-    for a in range(N_SMALL):
-        mixer_sides(a, 0)
     tok_swap = misc_hop(0, tok, tok2.at[0, :, mine_half], core_target)
-    tok_x = misc_hop(1, tok, tok2.at[1, :, mine_half], x_target)
-    pld_x = misc_hop(2, pld.at[:, span(1 - x, cw)], pld_v.at[1], x_target)
+
+    def tok_hop(n, target):
+        piece_rows = pl.ds(n % 2 * (rows // 2), rows // 2)
+        block = tok2.at[1, piece_rows, mine_half]
+        return misc_hop(1 + n if n < 2 else 0, tok.at[piece_rows, :] if n < 2 else block, block, target)
+
+    tok_x = [tok_hop(n, x_target) for n in range(2)]
+    tok_core = [tok_hop(n, core_target) for n in (2, 3)]
+    pld_x = misc_hop(3, pld.at[:, span(1 - x, cw)], pld_v.at[1], x_target)
     tok_swap.start()
-    pld_x.start()
-    pending += [tok_swap, tok_x, pld_x]
 
     own = [
         pltpu.make_async_copy(gup, gup_v, local.at[0]),
@@ -417,40 +440,56 @@
                 f = layer[k] * PLANE + p
                 z_hop(a, arrays[a][0](f), f, slot, land, to).start()
 
-        inner_pending.extend((a, slot) for a in range(N_SMALL))
-
-    def ffn_along_z(where):
-        @pl.when(inner == where)
-        def _():
-            for a in range(N_SMALL, N_BIG):
-                for k in range(1, LAYERS):
-                    z_hop(a, piece(a, layer[k]), fs, k, lands[k], k).start()
-
-    for k, to, land in ((1, 2, 3), (2, 1, 2), (3, 1, 3)):
+
+    def ffn_along_z(a):
+        for k in range(1, LAYERS):
+            z_hop(a, piece(a, layer[k]), fs, k, lands[k], k).start()
+
+    def mixer_step(k, to, land):
         for a in range(N_SMALL):
             z_done(a, k)
         relay(k, to, land, k + 1)
-        if k > 1:
-            ffn_along_z(k - 2)
+        for c in mixer_copies[k]:
+            c.start()
+
+    def mixer_corners(k):
         for a in range(N_SMALL):
-            mixer_sides(a, k)
-        if k == 1:
-            tok_x.start()
-        for a in range(N_SMALL):
-            mixer_corner(a, k - 1)
-    with jax.named_scope("tok_x"):
-        tok_x.wait_recv()
-    block = tok2.at[1, :, mine_half]
-    tok_core = misc_hop(3, block, block, core_target)
-    tok_core.start()
-    pending.append(tok_core)
+            mixer_corner(a, k)
+
+    mixer_corners(0)
+    pld_x.start()
+    mixer_step(1, 2, 3)
+
+    @pl.when(inner == 1)
+    def _():
+        mixer_step(2, 1, 2)
+
+    mixer_corners(1)
+    tok_x[0].start()
+
+    @pl.when(inner == 0)
+    def _():
+        mixer_step(2, 1, 2)
+        ffn_along_z(3)
+
+    mixer_corners(2)
+    tok_x[1].start()
+    mixer_step(3, 1, 3)
+
+    @pl.when(inner == 1)
+    def _():
+        ffn_along_z(3)
+
+    for n in range(2):
+        with jax.named_scope("tok_x"):
+            tok_x[n].wait_recv()
+        tok_core[n].start()
     for a in range(N_SMALL):
         mixer_corner(a, LAYERS - 1)
     sides(3, 0)
 
     with jax.named_scope("tokens"):
-        tok_swap.wait_recv()
-        tok_core.wait_recv()
+        arrival(tok2.at[0], AT_MISC).wait_recv()
         pld_x.wait_recv()
         own[2].wait()
 
@@ -461,9 +500,7 @@
     lax.fori_loop(0, 2, norm_step, 0)
     for c in own[3:]:
         c.wait()
-    for k in range(LAYERS):
-        for a in range(N_SMALL):
-            mixer_done(a, k)
+    mixer_done()
 
     def mixer_rows(r, _):
         place = position((rows, cw))
@@ -505,7 +542,11 @@
     mix_out[...] = (mix_keep[1] + mix_pair[1].astype(F32)).astype(BF16)
     mix_x = misc_hop(6, mix_out, mix_in, x_target)
     mix_x.start()
-    for k in range(1, LAYERS):
+    ffn_along_z(4)
+    z_done(3, 1)
+    sides(3, 1)
+    corners(3, 0)
+    for k in range(2, LAYERS):
         z_done(3, k)
         sides(3, k)
     with jax.named_scope("swap0"):
@@ -516,8 +557,6 @@
     after[:, mine_half] = (mix_keep[0] + mix_in[...].astype(F32)).astype(BF16)
     after_core = misc_hop(7, after.at[:, mine_half], after.at[:, mine_half], core_target)
     after_core.start()
-    pending += [mix_hop(0), mix_hop(1), mix_x, after_core]
-    corners(3, 0)
     with jax.named_scope("after"):
         after_core.wait_recv()
     n2[0] = normed_rows(after[...].astype(F32), gain2[...].astype(F32)[None, :])
@@ -525,16 +564,18 @@
 
     def rows_hop(k, land, slot, to):
         return hop(
-            n2.at[k, :, mine_half], n2.at[land, :, mine_half], n2_send.at[slot], n2_recv.at[land], line[to]
+            n2.at[k, :, mine_half],
+            n2.at[land, :, mine_half],
+            sent.at[ROWS_RELAY if slot else ROWS],
+            got.at[AT_ROWS + land],
+            line[to],
         )
 
     @pl.when(inner == 1)
     def _():
         rows_hop(0, 2, 1, 2).start()
 
-    c = rows_hop(0, 1, 0, 1)
-    c.start()
-    pending.append(c)
+    rows_hop(0, 1, 0, 1).start()
 
     def rows_arrived(k, to, land):
         with jax.named_scope(f"rows{k}"):
@@ -548,48 +589,84 @@
 
     def core_hop(k):
         block = n2.at[k, :, mine_half]
-        return hop(block, block, core_send.at[k], core_recv.at[k], core_target)
+        return hop(block, block, sent.at[ROWS], got.at[AT_CORE + k], core_target)
 
     corners(3, 1)
     rows_arrived(1, 2, 3)
     corners(3, 2)
-    rows_arrived(2, 1, 2)
+
+    @pl.when(inner == 1)
+    def _():
+        rows_arrived(2, 1, 2)
+
     corners(3, 3)
     z_done(4, 1)
     z_done(4, 2)
     down_a, down_b = down[0]
+    for block in down[0]:
+        sides(4, *block, kinds=(1,))
 
     @pl.when(inner == 1)
     def _():
         rows_arrived(3, 1, 3)
 
-    sides(4, *down_a)
-    sides(4, *down_b)
-
-    def up(k):
+    @pl.when(inner == 0)
+    def _():
+        rows_arrived(2, 1, 2)
+
+    block_rows = PLANE * deep
+
+    def up_dot(k, at, blocks):
+        total = None
+        for of in blocks:
+            where = span(layer[of], block_rows)
+            s = jnp.dot(n2[k, :, where], gu_all[where, at], preferred_element_type=F32)
+            total = s if total is None else total + s
+        return total
+
+    def up_early(k, _):
+        with jax.named_scope("up_early"):
+            for j in range(0, 2 * units, 4 * LANES):
+                at = slice(j, min(j + 4 * LANES, 2 * units))
+                part[k - 1, :, at] = up_dot(k, at, range(LAYERS - 1))
+        return 0
+
+    def up(k, late):
         place = position((rows, 4 * LANES))
         layer_taps = taps.at[z]
         width = gtaps.shape[0]
+
+        def halves(j, n):
+            at = slice(j, j + n)
+            if late:
+                s = part[k - 1, :, at] + up_dot(k, at, (LAYERS - 1,))
+            else:
+                s = jnp.dot(n2[k], gu_all[:, at], preferred_element_type=F32)
+            return rows_conv(s.astype(BF16).astype(F32), layer_taps[0:width, at], width, place[:, :n])
+
         j = 0
         while j < 2 * full * LANES:
             n = min(4 * LANES, 2 * full * LANES - j)
-            s = jnp.dot(n2[k], gu_all[:, j : j + n], preferred_element_type=F32)
-            s = rows_conv(s.astype(BF16).astype(F32), layer_taps[0:width, j : j + n], width, place[:, :n])
+            s = halves(j, n)
             for i in range(0, n, 2 * LANES):
                 g, v = s[:, i : i + LANES], s[:, i + LANES : i + 2 * LANES]
                 h = (j + i) // 2
                 hidden[k, :, h : h + LANES] = (g * jax.nn.sigmoid(g) * v).astype(BF16)
             j += n
         if rest:
-            s = jnp.dot(n2[k], gu_all[:, j:], preferred_element_type=F32)
-            s = rows_conv(s.astype(BF16).astype(F32), layer_taps[0:width, j:], width, place[:, :LANES])
+            s = halves(j, 2 * rest)
             h = s * jax.nn.sigmoid(s) * pltpu.roll(s, rest, 1)
             lane = lax.broadcasted_iota(jnp.int32, h.shape, 1)
             hidden[k, :, full * LANES : (full + 1) * LANES] = jnp.where(lane < rest, h, 0.0).astype(BF16)
 
     def up_step(k, _):
         with jax.named_scope("up"):
-            up(k)
+            up(k, False)
+        return 0
+
+    def up_late(k, _):
+        with jax.named_scope("up_late"):
+            up(k, True)
         return 0
 
     turn = (tp + z // 2) % 2
@@ -605,21 +682,23 @@
         return columns_of(j, True) % (half // quarter)
 
     def pair_hop(j, k):
-        return hop(give.at[j, k], pair.at[j, k], pair_send.at[j, k], pair_recv.at[j, k], core_target)
+        return hop(give.at[j, k], pair.at[j, k], sent.at[PAIR], got.at[AT_PAIR + j * LAYERS + k], core_target)
 
     def to_partner(j, k):
         landing = arrive.at[0, j] if k == 1 else joint.at[j, k - 2]
-        return hop(paired.at[j, k], landing, back_send.at[j, k], back_recv.at[j, k], line[1])
+        group = NEAR if k == 1 else FAR
+        return hop(paired.at[j, k], landing, sent.at[group], got.at[AT_BACK + j * LAYERS + k], line[1])
 
     def to_layer(j, k):
-        return hop(joint.at[j, k], arrive.at[1, j], joint_send.at[j, k], back_recv.at[j, 0], line[k + 2])
-
-    def part_sums(j, slots):
-        given, kept = span(columns_of(j, False), quarter), span(columns_of(j, True), quarter)
-        for k in slots:
+        return hop(joint.at[j, k], arrive.at[1, j], sent.at[FAR], got.at[AT_BACK + j * LAYERS], line[k + 2])
+
+    def part_sums(*parts):
+        for j, k in parts:
+            given = span(columns_of(j, False), quarter)
             give[j, k] = jnp.dot(hidden[k], dn_all[:, given], preferred_element_type=F32).astype(BF16)
             pair_hop(j, k).start()
-        for k in slots:
+        for j, k in parts:
+            kept = span(columns_of(j, True), quarter)
             keep = jnp.dot(hidden[k], dn_all[:, kept], preferred_element_type=F32)
             with jax.named_scope(f"pair{j}{k}"):
                 pair_hop(j, k).wait_recv()
@@ -641,47 +720,50 @@
             joint[j, k] = (joint[j, k].astype(F32) + paired[j, k + 2].astype(F32)).astype(BF16)
             to_layer(j, k).start()
 
-    for k in range(LAYERS):
-        corners_done(3, k)
+    corners_done(3, False)
+    for block in down[0]:
+        sides(4, *block, kinds=(2,))
     with jax.named_scope("across12"):
         core_hop(1).wait_recv()
         core_hop(2).wait_recv()
-    lax.fori_loop(1, 3, up_step, 0)
+    lax.fori_loop(1, 3, up_early, 0)
+    corners_done(3, True)
+    lax.fori_loop(1, 3, up_late, 0)
     corners(4, *down_a)
-    corners(4, *down_b)
+    corners(4, *down_b, kinds=(1,))
+    part_sums((0, 2), (0, 1))
+    corners(4, *down_b, kinds=(2,))
     z_done(4, 3)
     for block in down[1]:
         sides(4, *block)
-    part_sums(0, (2, 1))
-    for block in down[0]:
-        corners_done(4, *block)
-    part_sums(1, (2, 1))
 
     @pl.when(inner == 0)
     def _():
         rows_arrived(3, 1, 3)
 
+    corners_done(4, False)
+    part_sums((1, 2), (1, 1))
     with jax.named_scope("across3"):
         core_hop(3).wait_recv()
     lax.fori_loop(3, 4, up_step, 0)
-    part_sums(0, (3,))
-    part_sums(1, (3,))
+    part_sums((0, 3), (1, 3))
+    joint_sums(0, 0)
     corners(4, *down[1][0])
-    joint_sums(0, 0)
+    joint_sums(1, 0)
+    corners(4, *down[1][1], kinds=(1,))
+    part_sums((2, 3), (2, 2), (2, 1))
+    corners(4, *down[1][1], kinds=(2,))
+    joint_sums(0, 1)
+    corners_done(4, True)
+    part_sums((3, 3), (3, 2), (3, 1))
+    joint_sums(1, 1)
     lax.fori_loop(0, 1, up_step, 0)
-    corners(4, *down[1][1])
-    joint_sums(1, 0)
-    part_sums(2, (3, 2, 1))
-    joint_sums(0, 1)
-    for block in down[1]:
-        corners_done(4, *block)
-    part_sums(3, (3, 2, 1))
-    joint_sums(1, 1)
-    for j in range(LAYERS):
-        part_sums(j, (0,))
-    for j in (2, 3):
-        for k in (1, 0):
-            joint_sums(j, k)
+    part_sums((0, 0), (1, 0))
+    joint_sums(2, 1)
+    joint_sums(2, 0)
+    part_sums((2, 0), (3, 0))
+    joint_sums(3, 1)
+    joint_sums(3, 0)
 
     stores = []
     for j in range(LAYERS):
@@ -695,34 +777,31 @@
         stores.append(pltpu.make_async_copy(out_v.at[j], out.at[:, span(place_of(j), quarter)], local.at[j]))
         stores[j].start()
 
-    for c in pending + [core_hop(k) for k in range(1, LAYERS)]:
-        c.wait_send()
-    for a in range(N_SMALL, N_BIG):
-        for k in range(1, LAYERS):
-            z_hop(a, piece(a, z), fs, k, 1, k).wait_send()
-    for j in range(LAYERS):
-        to_partner(j, 1).wait_send()
-        for k in range(LAYERS):
-            pair_hop(j, k).wait_send()
-
-    @pl.when(inner == 0)
-    def _():
-        for j in range(LAYERS):
-            for k in (2, 3):
-                to_partner(j, k).wait_send()
-
-    @pl.when(inner == 1)
-    def _():
-        for a, slot in inner_pending:
-            z_hop(a, arrays[a][0](fs), fs, slot, 0, 1).wait_send()
-        for slot in range(1, LAYERS + 1):
-            rows_hop(0, 0, slot, 1).wait_send()
-        for j in range(LAYERS):
-            for k in range(2):
-                to_layer(j, k).wait_send()
-
-    for c in stores:
-        c.wait()
+    def all_sent(group, block):
+        hop(block, block, sent.at[group], got.at[0], core_target).wait_send()
+
+    with jax.named_scope("sent"):
+        every = slice(None)
+        all_sent(MIX, bo_all.at[pl.ds(0, 3 * N_SMALL * LAYERS * deep // 4), :])
+        all_sent(UP, gu_all.at[pl.ds(0, 3 * LAYERS * deep), :])
+        all_sent(DOWN, dn_all.at[pl.ds(0, units), pl.ds(0, 3 * LAYERS * wide)])
+        all_sent(MIX_Z, bo_all.at[pl.ds(0, N_SMALL * deep // 2), :])
+        all_sent(UP_Z, gu_all.at[pl.ds(0, 3 * deep), :])
+        all_sent(DOWN_Z, dn_all.at[pl.ds(0, units), pl.ds(0, 3 * wide)])
+        all_sent(ROWS, n2.at[pl.ds(0, 2)])
+        all_sent(MISC, bo_all.at[pl.ds(0, MISC_HALVES * rows * half // bo_all.shape[1] // 2), :])
+        all_sent(PAIR, give)
+        all_sent(NEAR, arrive.at[0])
+        all_sent(FAR, joint)
+
+        @pl.when(inner == 1)
+        def _():
+            all_sent(MIX_RELAY, bo_all.at[pl.ds(0, LAYERS * N_SMALL * deep // 2), :])
+            all_sent(ROWS_RELAY, n2.at[pl.ds(0, 2)])
+
+    with jax.named_scope("stores"):
+        for c in stores:
+            c.wait()
 
 
 def fused_layer(
@@ -781,20 +860,10 @@
         pltpu.VMEM((2, LAYERS, rows, quarter), BF16),
         pltpu.VMEM((LAYERS, 2, rows, quarter), BF16),
         pltpu.VMEM((LAYERS, rows, quarter), BF16),
-        dma((N_BIG, 5, LAYERS)),
-        dma((N_BIG, 5, LAYERS)),
-        dma((N_BIG, LAYERS + 1)),
+        pltpu.VMEM((2, rows, 2 * units), F32),
+        dma((N_SENT,)),
+        dma((AT_BACK + LAYERS * LAYERS,)),
         dma((8,)),
-        dma((16,)),
-        dma((LAYERS + 1,)),
-        dma((LAYERS,)),
-        dma((LAYERS,)),
-        dma((LAYERS,)),
-        dma((LAYERS, LAYERS)),
-        dma((LAYERS, LAYERS)),
-        dma((LAYERS, LAYERS)),
-        dma((LAYERS, LAYERS)),
-        dma((LAYERS, 2)),
     ]
     return pl.pallas_call(
         layer_kernel,

time: 158 us -> 154 us (0.975)
  Pallas kernels: 155 us -> 151 us
    pallas_call x1, Pallas kernels: 155 us -> 151 us  [fused_layer(): pl.pallas_call(layer_kernel, out_shape=jax.ShapeDtypeStruct((rows, half),...]
where the time goes in v3:
time: 154 us; the launch traced here: 153 us
  Pallas kernels  151 us (98%)
  local copies, waits for them, and re-layouts  1.87 us (1%)
    pallas_call x1, Pallas kernels, fused_layer(): pl.pallas_call(layer_kernel, out_shape=jax.ShapeDtypeStruct((rows, half),...  151 us

profile of v3, /device:TPU:0, one launch (start us, length us, event | category | flops | bytes accessed | tf_op | source)
XLA Modules:
  0.0 152.6 jit_solution(11950297370008331455)
XLA Ops:
  0.0 150.8 %layer.1 = bf16[256,1024]{1,0:T(8,128)(2,1)} custom-call(bf16[256,1024]{1,0:T(8,128)(2,1)} %tok.1, bf16[2048]{0:T(1024)(128)(2,1)} %gain1.1, bf16[128,512]{1,0:T(8,128)(2,1)} %rb.1, bf16[128,512]{1,0:T(8,128)(2,1)} %og.1, bf16[4,512]{1,0:T(4,128)(2,1)} %ctaps.1, bf16[8,64,64]{2,1,0:T(8,128)(2,1)} %rmap.1, bf16[8,64,64]{2,1,0:T(8,128)(2,1)} %imap.1, ...), custom_call_target="tpu_custom_call" | custom-call | tf_op jit(solution)/shard_map/layer/pallas_call | solution.py:868
  150.8 1.9 %copy.18 = bf16[256,1024]{1,0:T(8,128)(2,1)} copy(bf16[256,1024]{1,0:T(8,128)(2,1)} %layer.1) | data formatting | bytes 1048576

commit v4 on v3

--- a/solution.py
+++ b/solution.py
@@ -144,7 +144,7 @@
 F32, BF16 = jnp.float32, jnp.bfloat16
 N_SMALL, N_BIG = 3, 5
 ROWS_CUT = 6
-MISC_HALVES = 15
+MISC_QUARTERS = 29
 N_SENT = 13
 AT_Z = 0
 AT_MIX = AT_Z + N_BIG * LAYERS
@@ -239,7 +239,7 @@
     tok, gain1, rb, og, ctaps, rmap, imap, rate, pld, mo, gain2, gup, vup, gtaps, vtaps, dn,
     out,
     tok2, bo_all, mo_all, gup_v, vup_v, stage, gu_all, dn_all, taps, gmap, pld_v,
-    normed, mix_give, mix_keep, mix_pair, mix_out, mix_in, after, n2, hidden, give, pair, paired, arrive, joint, out_v, part,
+    normed, mix_give, mix_keep, mix_pair, mix_out, mix_in, after, n2, hidden, give, pair, paired, arrive, joint, out_v, part, pld_b,
     sent, got, local,
 ):
     fs, tp = lax.axis_index("fs"), lax.axis_index("tp")
@@ -385,7 +385,7 @@
 
     tok_x = [tok_hop(n, x_target) for n in range(2)]
     tok_core = [tok_hop(n, core_target) for n in (2, 3)]
-    pld_x = misc_hop(3, pld.at[:, span(1 - x, cw)], pld_v.at[1], x_target)
+    pld_x = misc_hop(3, pld_b.at[0], pld_b.at[1], x_target)
     tok_swap.start()
 
     own = [
@@ -397,10 +397,13 @@
         pltpu.make_async_copy(og, arrays[1][0](fs), local.at[5]),
         pltpu.make_async_copy(mo, arrays[2][0](fs), local.at[6]),
         pltpu.make_async_copy(piece(4, z), arrays[4][0](fs), local.at[7]),
+        pltpu.make_async_copy(pld.at[:, span(1 - x, cw)], pld_v.at[1], local.at[8]),
     ]
     for c in own:
         c.start()
 
+    own[8].wait()
+    pld_b[0] = pld_v[1].astype(BF16)
     own[0].wait()
     own[1].wait()
 
@@ -491,6 +494,8 @@
     with jax.named_scope("tokens"):
         arrival(tok2.at[0], AT_MISC).wait_recv()
         pld_x.wait_recv()
+    pld_v[1] = pld_b[1].astype(F32)
+    with jax.named_scope("tokens"):
         own[2].wait()
 
     def norm_step(r, _):
@@ -498,7 +503,7 @@
         return 0
 
     lax.fori_loop(0, 2, norm_step, 0)
-    for c in own[3:]:
+    for c in own[3:8]:
         c.wait()
     mixer_done()
 
@@ -729,11 +734,13 @@
     lax.fori_loop(1, 3, up_early, 0)
     corners_done(3, True)
     lax.fori_loop(1, 3, up_late, 0)
-    corners(4, *down_a)
-    corners(4, *down_b, kinds=(1,))
-    part_sums((0, 2), (0, 1))
+    z_done(4, 3)
+    for block in down[0]:
+        corners(4, *block, kinds=(1,))
+    part_sums((0, 2))
+    corners(4, *down_a, kinds=(2,))
+    part_sums((0, 1))
     corners(4, *down_b, kinds=(2,))
-    z_done(4, 3)
     for block in down[1]:
         sides(4, *block)
 
@@ -741,29 +748,29 @@
     def _():
         rows_arrived(3, 1, 3)
 
-    corners_done(4, False)
-    part_sums((1, 2), (1, 1))
     with jax.named_scope("across3"):
         core_hop(3).wait_recv()
     lax.fori_loop(3, 4, up_step, 0)
-    part_sums((0, 3), (1, 3))
+    part_sums((0, 3))
+    corners_done(4, False)
+    part_sums((1, 2), (1, 1), (1, 3))
     joint_sums(0, 0)
     corners(4, *down[1][0])
-    joint_sums(1, 0)
     corners(4, *down[1][1], kinds=(1,))
     part_sums((2, 3), (2, 2), (2, 1))
     corners(4, *down[1][1], kinds=(2,))
     joint_sums(0, 1)
+    joint_sums(1, 0)
     corners_done(4, True)
     part_sums((3, 3), (3, 2), (3, 1))
     joint_sums(1, 1)
+    joint_sums(2, 1)
     lax.fori_loop(0, 1, up_step, 0)
+    joint_sums(2, 0)
     part_sums((0, 0), (1, 0))
-    joint_sums(2, 1)
-    joint_sums(2, 0)
-    part_sums((2, 0), (3, 0))
     joint_sums(3, 1)
     joint_sums(3, 0)
+    part_sums((2, 0), (3, 0))
 
     stores = []
     for j in range(LAYERS):
@@ -789,7 +796,7 @@
         all_sent(UP_Z, gu_all.at[pl.ds(0, 3 * deep), :])
         all_sent(DOWN_Z, dn_all.at[pl.ds(0, units), pl.ds(0, 3 * wide)])
         all_sent(ROWS, n2.at[pl.ds(0, 2)])
-        all_sent(MISC, bo_all.at[pl.ds(0, MISC_HALVES * rows * half // bo_all.shape[1] // 2), :])
+        all_sent(MISC, bo_all.at[pl.ds(0, MISC_QUARTERS * rows * half // bo_all.shape[1] // 4), :])
         all_sent(PAIR, give)
         all_sent(NEAR, arrive.at[0])
         all_sent(FAR, joint)
@@ -861,9 +868,10 @@
         pltpu.VMEM((LAYERS, 2, rows, quarter), BF16),
         pltpu.VMEM((LAYERS, rows, quarter), BF16),
         pltpu.VMEM((2, rows, 2 * units), F32),
+        pltpu.VMEM((2, rows, cw), BF16),
         dma((N_SENT,)),
         dma((AT_BACK + LAYERS * LAYERS,)),
-        dma((8,)),
+        dma((9,)),
     ]
     return pl.pallas_call(
         layer_kernel,

time: 154 us -> 151 us (0.981)
  Pallas kernels: 151 us -> 149 us
    pallas_call x1, Pallas kernels: 151 us -> 149 us  [fused_layer(): pl.pallas_call(layer_kernel, out_shape=jax.ShapeDtypeStruct((rows, half),...]
where the time goes in v4:
time: 151 us
  Pallas kernels  149 us (99%)
  local copies, waits for them, and re-layouts  1.87 us (1%)
    pallas_call x1, Pallas kernels, fused_layer(): pl.pallas_call(layer_kernel, out_shape=jax.ShapeDtypeStruct((rows, half),...  149 us

profile of v4, /device:TPU:0, one launch (start us, length us, event | category | flops | bytes accessed | tf_op | source)
XLA Modules:
  0.0 150.7 jit_solution(5746111711575524653)
XLA Ops:
  0.0 148.8 %layer.1 = bf16[256,1024]{1,0:T(8,128)(2,1)} custom-call(bf16[256,1024]{1,0:T(8,128)(2,1)} %tok.1, bf16[2048]{0:T(1024)(128)(2,1)} %gain1.1, bf16[128,512]{1,0:T(8,128)(2,1)} %rb.1, bf16[128,512]{1,0:T(8,128)(2,1)} %og.1, bf16[4,512]{1,0:T(4,128)(2,1)} %ctaps.1, bf16[8,64,64]{2,1,0:T(8,128)(2,1)} %rmap.1, bf16[8,64,64]{2,1,0:T(8,128)(2,1)} %imap.1, ...), custom_call_target="tpu_custom_call" | custom-call | tf_op jit(solution)/shard_map/layer/pallas_call | solution.py:876
  148.8 1.9 %copy.18 = bf16[256,1024]{1,0:T(8,128)(2,1)} copy(bf16[256,1024]{1,0:T(8,128)(2,1)} %layer.1) | data formatting | bytes 1048576

commit v5 on v4

--- a/solution.py
+++ b/solution.py
@@ -762,14 +762,14 @@
     joint_sums(0, 1)
     joint_sums(1, 0)
     corners_done(4, True)
-    part_sums((3, 3), (3, 2), (3, 1))
+    part_sums((3, 2), (3, 3), (3, 1))
     joint_sums(1, 1)
     joint_sums(2, 1)
     lax.fori_loop(0, 1, up_step, 0)
     joint_sums(2, 0)
     part_sums((0, 0), (1, 0))
+    joint_sums(3, 0)
     joint_sums(3, 1)
-    joint_sums(3, 0)
     part_sums((2, 0), (3, 0))
 
     stores = []

time: 151 us -> 154 us (1.020)
  Pallas kernels: 149 us -> 152 us
    pallas_call x1, Pallas kernels: 149 us -> 152 us  [fused_layer(): pl.pallas_call(layer_kernel, out_shape=jax.ShapeDtypeStruct((rows, half),...]
where the time goes in v5:
time: 154 us; the launch traced here: 153 us
  Pallas kernels  152 us (99%)
  local copies, waits for them, and re-layouts  1.87 us (1%)
    pallas_call x1, Pallas kernels, fused_layer(): pl.pallas_call(layer_kernel, out_shape=jax.ShapeDtypeStruct((rows, half),...  152 us

profile of v5, /device:TPU:0, one launch (start us, length us, event | category | flops | bytes accessed | tf_op | source)
XLA Modules:
  0.0 153.5 jit_solution(17637928062198056960)
XLA Ops:
  0.0 151.6 %layer.1 = bf16[256,1024]{1,0:T(8,128)(2,1)} custom-call(bf16[256,1024]{1,0:T(8,128)(2,1)} %tok.1, bf16[2048]{0:T(1024)(128)(2,1)} %gain1.1, bf16[128,512]{1,0:T(8,128)(2,1)} %rb.1, bf16[128,512]{1,0:T(8,128)(2,1)} %og.1, bf16[4,512]{1,0:T(4,128)(2,1)} %ctaps.1, bf16[8,64,64]{2,1,0:T(8,128)(2,1)} %rmap.1, bf16[8,64,64]{2,1,0:T(8,128)(2,1)} %imap.1, ...), custom_call_target="tpu_custom_call" | custom-call | tf_op jit(solution)/shard_map/layer/pallas_call | solution.py:876
  151.6 1.9 %copy.18 = bf16[256,1024]{1,0:T(8,128)(2,1)} copy(bf16[256,1024]{1,0:T(8,128)(2,1)} %layer.1) | data formatting | bytes 1048576
